TPU v7x, 32 devices: a whole 2x2x4 slice. The times are simulated.
32 devices in a mesh: sp: 8 (over z, y), tp: 4 (over x, core).
Axes of the slice: x: 2, y: 2, z: 4, core: 2. Of those that a mesh axis runs over, the one named last changes fastest.
Arguments:
- tokens: bfloat16 [3072, 2048], P('sp', 'tp'), may hold values from -6 to 6
- norm_gain: float32 [2048], replicated, may hold values from 0.1 to 1.9
- w_glu_value: bfloat16 [2048, 2048], P(None, 'tp'), may hold values from -0.125 to 0.125
- w_glu_gate: bfloat16 [2048, 2048], P(None, 'tp'), may hold values from -0.125 to 0.125
- w_query: bfloat16 [2048, 2048], P(None, 'tp'), may hold values from -0.125 to 0.125
- w_key: bfloat16 [2048, 2048], P(None, 'tp'), may hold values from -0.125 to 0.125
- w_value: bfloat16 [2048, 2048], P(None, 'tp'), may hold values from -0.125 to 0.125
- score_offset: float32 [32], P('tp'), may hold values from -15 to -4, as said below
- conv_taps: bfloat16 [31, 2048], P(None, 'tp'), may hold values from -1 to 1
- conv_gain: float32 [2048], replicated, may hold values from 0.1 to 1.9
- w_conv_out: bfloat16 [2048, 2048], P(None, 'tp'), may hold values from -0.125 to 0.125
- w_attn_out: bfloat16 [2048, 2048], P(None, 'tp'), may hold values from -1 to 1
- w_gate_conv: bfloat16 [2048, 2048], P(None, 'tp'), may hold values from -0.125 to 0.125
- w_gate_attn: bfloat16 [2048, 2048], P(None, 'tp'), may hold values from -0.125 to 0.125
Outputs:
- mixed: bfloat16 [3072, 2048], P('sp', 'tp')
- log_weight: float32 [32, 3072], P('tp', 'sp')
Inputs may be any that keep to these rules, and one draw needn't show every extreme that they name: `score_offset`: per-head score offsets.
All inputs are finite; a program needn't handle non-finite values.
Results may differ from a plain program's by a relative error of at most 0.0078.
Values may be sent and summed in bfloat16 or wider, within the bound.
A program may use at most 128 MiB of HBM per device.

v0:
```python
import jax
import jax.numpy as jnp
from jax import lax
from jax.sharding import PartitionSpec as P

HEAD = 64
WIDTH = 31


key_span = 512


def passed_along(array, axis, by):
    length = lax.axis_size(axis)
    pairs = [(i, i + by) for i in range(length) if 0 <= i + by < length]
    return lax.ppermute(array, axis, pairs)


def sweep_block(
    sweep_state, key_block, value_block, key_first, query_first, query_heads, offsets, score_scale
):
    summed, spent_stick = sweep_state
    head_count = offsets.shape[0]
    query_count = query_heads.shape[0]
    key_count = key_block.shape[0]
    key_heads = key_block.reshape(key_count, head_count, -1)
    value_heads = value_block.reshape(key_count, head_count, -1)
    scores = (
        jnp.einsum("thd,shd->hts", query_heads, key_heads, preferred_element_type=jnp.float32)
        * score_scale
        + offsets[:, None, None]
    )
    query_pos = query_first + lax.iota(jnp.int32, query_count)
    key_pos = key_first + lax.iota(jnp.int32, key_count)
    allowed = (key_pos[None, :] <= query_pos[:, None]) & (key_pos[None, :] >= 0)
    softened = jnp.where(allowed[None], jax.nn.softplus(scores), 0.0)
    behind = lax.cumsum(softened, axis=2, reverse=True)
    stick = jnp.where(
        allowed[None], jnp.exp(scores - behind - spent_stick[:, :, None]), 0.0
    ).astype(jnp.bfloat16)
    summed = summed + jnp.einsum(
        "hts,shd->thd", stick, value_heads, preferred_element_type=jnp.float32
    )
    return (summed, spent_stick + behind[:, :, 0])


def body(
    tokens,
    norm_gain,
    w_glu_value,
    w_glu_gate,
    w_query,
    w_key,
    w_value,
    score_offset,
    conv_taps,
    conv_gain,
    w_conv_out,
    w_attn_out,
    w_gate_conv,
    w_gate_attn,
):
    whole_rows = lax.all_gather(tokens, "tp", axis=1, tiled=True)
    features = whole_rows.astype(jnp.float32)
    normed = (
        features
        * lax.rsqrt(jnp.mean(features * features, axis=-1, keepdims=True) + 1e-06)
        * norm_gain
    ).astype(jnp.bfloat16)
    glued = (
        jnp.dot(normed, w_glu_value, preferred_element_type=jnp.float32)
        * jax.nn.sigmoid(jnp.dot(normed, w_glu_gate, preferred_element_type=jnp.float32))
    ).astype(jnp.bfloat16)
    queries = jnp.dot(normed, w_query, preferred_element_type=jnp.float32).astype(jnp.bfloat16)
    keys = jnp.dot(normed, w_key, preferred_element_type=jnp.float32).astype(jnp.bfloat16)
    values = jnp.dot(normed, w_value, preferred_element_type=jnp.float32).astype(jnp.bfloat16)
    tok_rows = whole_rows.shape[0]
    tap_count = conv_taps.shape[0]
    channels = glued.shape[1]
    previous = passed_along(glued[tok_rows - (tap_count - 1) :], "sp", 1)
    extended = jnp.concatenate([previous, glued], axis=0)
    tap_rows = conv_taps.astype(jnp.float32)
    convolved = jnp.zeros((tok_rows, channels), jnp.float32)
    for tap in range(WIDTH):
        convolved = convolved + tap_rows[tap] * extended[tap : tap + tok_rows].astype(jnp.float32)
    convolved = convolved.astype(jnp.bfloat16)
    head_count = score_offset.shape[0]
    head_width = queries.shape[1] // head_count
    score_scale = 1.0 / HEAD**0.5
    query_heads = queries.reshape(tok_rows, head_count, head_width)
    own_index = lax.axis_index("sp")
    query_first = own_index * tok_rows
    start_state = (
        jnp.zeros((tok_rows, head_count, head_width), jnp.float32),
        jnp.zeros((head_count, tok_rows), jnp.float32),
    )
    gathered = (
        lax.all_gather(keys, "sp", axis=0, tiled=True),
        lax.all_gather(values, "sp", axis=0, tiled=True),
    )
    leading = jnp.zeros((key_span, keys.shape[1]), jnp.bfloat16)
    all_keys = jnp.concatenate([leading, gathered[0]], axis=0)
    all_values = jnp.concatenate([leading, gathered[1]], axis=0)
    key_end = (own_index + 1) * tok_rows
    turns = (key_end + key_span - 1) // key_span

    def advance(turn_index, sweep_state):
        key_first = key_end - (turn_index + 1) * key_span
        key_block = lax.dynamic_slice_in_dim(all_keys, key_first + key_span, key_span, 0)
        value_block = lax.dynamic_slice_in_dim(all_values, key_first + key_span, key_span, 0)
        return sweep_block(
            sweep_state,
            key_block,
            value_block,
            key_first,
            query_first,
            query_heads,
            score_offset,
            score_scale,
        )

    summed, spent_stick = lax.fori_loop(0, turns, advance, start_state)
    attended = summed.reshape(tok_rows, head_count * head_width).astype(jnp.bfloat16)
    log_weight = jnp.log(-jnp.expm1(-spent_stick))
    gate_conv = jax.nn.sigmoid(jnp.dot(normed, w_gate_conv, preferred_element_type=jnp.float32))
    gate_attn = jax.nn.sigmoid(jnp.dot(normed, w_gate_attn, preferred_element_type=jnp.float32))
    all_channels = conv_gain.shape[0]
    conv_float = convolved.astype(jnp.float32)
    channel_sum, channel_squares = lax.psum(
        (
            jnp.sum(conv_float, axis=-1, keepdims=True),
            jnp.sum(conv_float * conv_float, axis=-1, keepdims=True),
        ),
        "tp",
    )
    channel_mean = channel_sum / all_channels
    channel_var = channel_squares / all_channels - channel_mean * channel_mean
    local_gain = lax.dynamic_slice_in_dim(conv_gain, lax.axis_index("tp") * channels, channels, 0)
    conv_act = jax.nn.silu(
        (conv_float - channel_mean) * lax.rsqrt(channel_var + 1e-05) * local_gain
    ).astype(jnp.bfloat16)
    conv_piece = lax.all_gather(conv_act, "tp", axis=1, tiled=True)
    attn_piece = lax.all_gather(attended, "tp", axis=1, tiled=True)
    conv_branch = jnp.dot(conv_piece, w_conv_out, preferred_element_type=jnp.float32)
    attn_branch = jnp.dot(attn_piece, w_attn_out, preferred_element_type=jnp.float32)
    mixed = (gate_conv * conv_branch + gate_attn * attn_branch).astype(jnp.bfloat16)
    return (mixed, log_weight)


def solution(mesh):
    in_specs = (
        P("sp", "tp"),
        P(),
        P(None, "tp"),
        P(None, "tp"),
        P(None, "tp"),
        P(None, "tp"),
        P(None, "tp"),
        P("tp"),
        P(None, "tp"),
        P(),
        P(None, "tp"),
        P(None, "tp"),
        P(None, "tp"),
        P(None, "tp"),
    )
    out_specs = (P("sp", "tp"), P("tp", "sp"))
    return jax.shard_map(body, mesh=mesh, in_specs=in_specs, out_specs=out_specs, check_vma=False)
```

profile of v0, /device:TPU:29, one launch (start us, length us, event | category | flops | bytes accessed | tf_op | source)
XLA Modules:
  0.0 367.0 jit_solution(1898526458880367663)
XLA Ops:
  7.2 0.7 all-gather.6.cloned.1.call-update
  8.0 22.6 %all-gather.6.cloned.1.call-done = bf16[384,2048]{1,0:T(8,128)(2,1)} async-done(((bf16[384,512]{1,0:T(8,128)(2,1)}), bf16[384,2048]{1,0:T(8,128)(2,1)}) %all-gather.6.cloned.1.call-update) | async-done | bytes 1572880 | tf_op jit(solution)/shard_map/all_gather | solution.py:63
  30.5 1.8 fusion.22
  32.4 3.2 convolution_convert_fusion.2
  35.6 4.0 %convolution_convert_fusion.1 = bf16[384,512]{1,0:T(8,128)(2,1)} fusion(bf16[2048,512]{1,0:T(8,128)(2,1)} %param.21, bf16[384,2048]{1,0:T(8,128)(2,1)} %all-gather.6.cloned.1.call-done, f32[2048]{0:T(1024)S(1)} %copy-done.8, f32[384]{0:T(512)S(1)} %add_rsqrt_fusion), kind=kOutput, calls=%fused_computation.84 | convolution fusion | flops 808648704 | bytes 4072960 | tf_op jit(solution)/shard_map/dot_general | solution.py:75
  39.7 2.6 convolution_convert_fusion
  42.5 50.4 %all-gather.10.cloned.1.call-done = bf16[3072,512]{1,0:T(8,128)(2,1)} async-done(((bf16[384,512]{1,0:T(8,128)(2,1)}), bf16[3072,512]{1,0:T(8,128)(2,1)}) %all-gather.10.cloned.1.call-update) | async-done | bytes 3145744 | tf_op jit(solution)/shard_map/all_gather | solution.py:99
  92.9 3.9 %concatenate.10 = bf16[3584,512]{1,0:T(8,128)(2,1)} pad(bf16[3072,512]{1,0:T(8,128)(2,1)} %all-gather.10.cloned.1.call-done, bf16[]{:T(256)} %constant.89.clone.1), padding=512_0x0_0 | pad | bytes 6815746 | tf_op jit(solution)/shard_map/concatenate | solution.py:103
  96.8 57.0 %all-gather.12.cloned.1.call-done = bf16[3072,512]{1,0:T(8,128)(2,1)} async-done(((bf16[384,512]{1,0:T(8,128)(2,1)}), bf16[3072,512]{1,0:T(8,128)(2,1)}) %all-gather.12.cloned.1.call-update) | async-done | bytes 3145744 | tf_op jit(solution)/shard_map/all_gather | solution.py:98
  153.8 3.9 %concatenate.11 = bf16[3584,512]{1,0:T(8,128)(2,1)} pad(bf16[3072,512]{1,0:T(8,128)(2,1)} %all-gather.12.cloned.1.call-done, bf16[]{:T(256)} %constant.89.clone.1), padding=512_0x0_0 | pad | bytes 6815746 | tf_op jit(solution)/shard_map/concatenate | solution.py:102
  157.8 154.0 %while.14 = (s32[]{:T(128)}, f32[384,8,64]{0,2,1:T(8,128)S(1)}, f32[8,384]{1,0:T(8,128)S(1)}, s32[]{:T(128)}, s32[]{:T(128)}, /*index=5*/bf16[3584,512]{1,0:T(8,...) while((s32[]{:T(128)}, f32[384,8,64]{0,2,1:T(8,128)S(1)}, ...), condition=%wide.region_8.9_spmd, body=%wide.region_5.8_spmd.sunk | while | flops 628213632 | bytes 71053592 | solution.py:122
  158.1 1.3 constant_dynamic-slice_fusion.3
  159.3 0.2 copy.42
  160.0 4.7 %fusion.112 = (f32[8,384,512]{1,2,0:T(8,128)S(1)}, f32[8,512,384]{2,1,0:T(8,128)S(1)}) fusion(f32[8]{0:T(128)S(1)} %get-tuple-element.322, pred[384,512]{0,1:T(8,128)(4,1)S(1)} %compare_and_fusion.2, bf16[512,8,64]{0,2,1:T(8,128)(2,1)S(1)} %bitcast.118, bf16[384,8,64]{0,2,1:T(8,128)(2,1)S(1)} %get-tuple-element.321), kind=kOutput, calls=%fused_computation.1.clone.1 | convolution fusion | flops 215482368 | bytes 13697056 | tf_op jit(solution)/shard_map/while/body/thd,shd->hts/dot_general | solution.py:29
  164.7 15.1 %fusion.113 = f32[8,384,4,128]{1,0,3,2:T(8,128)S(1)} fusion(f32[8,384,4,128]{1,3,2,0:T(8,128)S(1)} %bitcast.116), kind=kOutput, calls=%fused_computation.13.clone.1 | output fusion | flops 199753728 | bytes 12582912 | tf_op jit(solution)/shard_map/reduce-window.6
  180.0 0.4 broadcast_add_fusion.2
  180.4 1.2 copy.44
  181.6 2.0 fusion.115
  183.7 1.3 constant_dynamic-slice_fusion.3
  185.6 4.7 %fusion.112 = (f32[8,384,512]{1,2,0:T(8,128)S(1)}, f32[8,512,384]{2,1,0:T(8,128)S(1)}) fusion(f32[8]{0:T(128)S(1)} %get-tuple-element.322, pred[384,512]{0,1:T(8,128)(4,1)S(1)} %compare_and_fusion.2, bf16[512,8,64]{0,2,1:T(8,128)(2,1)S(1)} %bitcast.118, bf16[384,8,64]{0,2,1:T(8,128)(2,1)S(1)} %get-tuple-element.321), kind=kOutput, calls=%fused_computation.1.clone.1 | convolution fusion | flops 215482368 | bytes 13697056 | tf_op jit(solution)/shard_map/while/body/thd,shd->hts/dot_general | solution.py:29
  190.4 15.1 %fusion.113 = f32[8,384,4,128]{1,0,3,2:T(8,128)S(1)} fusion(f32[8,384,4,128]{1,3,2,0:T(8,128)S(1)} %bitcast.116), kind=kOutput, calls=%fused_computation.13.clone.1 | output fusion | flops 199753728 | bytes 12582912 | tf_op jit(solution)/shard_map/reduce-window.6
  205.6 0.4 broadcast_add_fusion.2
  206.0 1.2 copy.44
  207.2 2.0 fusion.115
  209.3 1.3 constant_dynamic-slice_fusion.3
  211.3 4.7 %fusion.112 = (f32[8,384,512]{1,2,0:T(8,128)S(1)}, f32[8,512,384]{2,1,0:T(8,128)S(1)}) fusion(f32[8]{0:T(128)S(1)} %get-tuple-element.322, pred[384,512]{0,1:T(8,128)(4,1)S(1)} %compare_and_fusion.2, bf16[512,8,64]{0,2,1:T(8,128)(2,1)S(1)} %bitcast.118, bf16[384,8,64]{0,2,1:T(8,128)(2,1)S(1)} %get-tuple-element.321), kind=kOutput, calls=%fused_computation.1.clone.1 | convolution fusion | flops 215482368 | bytes 13697056 | tf_op jit(solution)/shard_map/while/body/thd,shd->hts/dot_general | solution.py:29
  216.0 15.1 %fusion.113 = f32[8,384,4,128]{1,0,3,2:T(8,128)S(1)} fusion(f32[8,384,4,128]{1,3,2,0:T(8,128)S(1)} %bitcast.116), kind=kOutput, calls=%fused_computation.13.clone.1 | output fusion | flops 199753728 | bytes 12582912 | tf_op jit(solution)/shard_map/reduce-window.6
  231.2 0.4 broadcast_add_fusion.2
  231.7 1.2 copy.44
  232.9 2.0 fusion.115
  234.9 1.3 constant_dynamic-slice_fusion.3
  236.9 4.7 %fusion.112 = (f32[8,384,512]{1,2,0:T(8,128)S(1)}, f32[8,512,384]{2,1,0:T(8,128)S(1)}) fusion(f32[8]{0:T(128)S(1)} %get-tuple-element.322, pred[384,512]{0,1:T(8,128)(4,1)S(1)} %compare_and_fusion.2, bf16[512,8,64]{0,2,1:T(8,128)(2,1)S(1)} %bitcast.118, bf16[384,8,64]{0,2,1:T(8,128)(2,1)S(1)} %get-tuple-element.321), kind=kOutput, calls=%fused_computation.1.clone.1 | convolution fusion | flops 215482368 | bytes 13697056 | tf_op jit(solution)/shard_map/while/body/thd,shd->hts/dot_general | solution.py:29
  241.6 15.1 %fusion.113 = f32[8,384,4,128]{1,0,3,2:T(8,128)S(1)} fusion(f32[8,384,4,128]{1,3,2,0:T(8,128)S(1)} %bitcast.116), kind=kOutput, calls=%fused_computation.13.clone.1 | output fusion | flops 199753728 | bytes 12582912 | tf_op jit(solution)/shard_map/reduce-window.6
  256.9 0.4 broadcast_add_fusion.2
  257.3 1.2 copy.44
  258.5 2.0 fusion.115
  260.6 1.3 constant_dynamic-slice_fusion.3
  262.5 4.7 %fusion.112 = (f32[8,384,512]{1,2,0:T(8,128)S(1)}, f32[8,512,384]{2,1,0:T(8,128)S(1)}) fusion(f32[8]{0:T(128)S(1)} %get-tuple-element.322, pred[384,512]{0,1:T(8,128)(4,1)S(1)} %compare_and_fusion.2, bf16[512,8,64]{0,2,1:T(8,128)(2,1)S(1)} %bitcast.118, bf16[384,8,64]{0,2,1:T(8,128)(2,1)S(1)} %get-tuple-element.321), kind=kOutput, calls=%fused_computation.1.clone.1 | convolution fusion | flops 215482368 | bytes 13697056 | tf_op jit(solution)/shard_map/while/body/thd,shd->hts/dot_general | solution.py:29
  267.2 15.1 %fusion.113 = f32[8,384,4,128]{1,0,3,2:T(8,128)S(1)} fusion(f32[8,384,4,128]{1,3,2,0:T(8,128)S(1)} %bitcast.116), kind=kOutput, calls=%fused_computation.13.clone.1 | output fusion | flops 199753728 | bytes 12582912 | tf_op jit(solution)/shard_map/reduce-window.6
  282.5 0.4 broadcast_add_fusion.2
  282.9 1.2 copy.44
  284.1 2.0 fusion.115
  286.2 1.3 constant_dynamic-slice_fusion.3
  288.2 4.7 %fusion.112 = (f32[8,384,512]{1,2,0:T(8,128)S(1)}, f32[8,512,384]{2,1,0:T(8,128)S(1)}) fusion(f32[8]{0:T(128)S(1)} %get-tuple-element.322, pred[384,512]{0,1:T(8,128)(4,1)S(1)} %compare_and_fusion.2, bf16[512,8,64]{0,2,1:T(8,128)(2,1)S(1)} %bitcast.118, bf16[384,8,64]{0,2,1:T(8,128)(2,1)S(1)} %get-tuple-element.321), kind=kOutput, calls=%fused_computation.1.clone.1 | convolution fusion | flops 215482368 | bytes 13697056 | tf_op jit(solution)/shard_map/while/body/thd,shd->hts/dot_general | solution.py:29
  292.9 15.1 %fusion.113 = f32[8,384,4,128]{1,0,3,2:T(8,128)S(1)} fusion(f32[8,384,4,128]{1,3,2,0:T(8,128)S(1)} %bitcast.116), kind=kOutput, calls=%fused_computation.13.clone.1 | output fusion | flops 199753728 | bytes 12582912 | tf_op jit(solution)/shard_map/reduce-window.6
  308.1 0.4 broadcast_add_fusion.2
  308.5 1.2 copy.44
  309.8 2.0 fusion.115
  311.8 0.8 convert_element_type.179
  312.6 0.3 all-gather.8.cloned.1.call-start
  313.0 3.4 fusion.31
  316.4 1.0 fusion.35
  317.4 1.3 collective-permute-start
  318.7 0.8 dynamic_slice.15
  319.5 2.6 collective-permute-done
  322.1 3.7 %convert_reduce_fusion = (f32[384]{0:T(512)S(1)}, f32[384]{0:T(512)S(1)}, bf16[384,512]{1,0:T(8,128)(2,1)S(1)}) fusion(bf16[384,512]{1,0:T(8,128)(2,1)S(1)} %fusion.35, f32[512]{0:T(512)S(1)} %bitcast.151, bf16[30,512]{1,0:T(8,128)(2,1)S(1)} %collective-permute-done, f32[512]{0:T(512)S(1)} %bitcast.150, f32[512]{0:T(512)S(1)} %bitcast.149, ...), kind=kLoop, calls=%fused_computation.88 | loop fusion | flops 36764928 | bytes 883712 | tf_op jit(solution)/shard_map/reduce_sum | solution.py:131
  325.8 7.3 %all-reduce.2 = (f32[384,1]{0,1:T(1,128)S(1)}, f32[384,1]{0,1:T(1,128)S(1)}) all-reduce(f32[384,1]{0,1:T(1,128)S(1)} %broadcast_in_dim.41, f32[384,1]{0,1:T(1,128)S(1)} %broadcast_in_dim.42), channel_id=1, replica_groups=mesh['sp'=8,'tp'=4] {'tp'}, use_global_device_ids=true, to_apply=%region_2.3 | all-reduce | flops 768 | bytes 6144 | tf_op jit(solution)/shard_map/psum | solution.py:129
  333.1 1.1 fusion.44
  334.3 2.9 fusion.33
  337.2 2.0 fusion.29
  339.2 0.6 negate_log_fusion
  339.8 4.1 %convolution_multiply_fusion = f32[384,512]{1,0:T(8,128)} fusion(f32[384,512]{1,0:T(8,128)S(1)} %fusion.33, bf16[384,2048]{0,1:T(8,128)(2,1)} %all-gather.14.cloned.1.call-done, bf16[2048,512]{1,0:T(8,128)(2,1)} %param.27), kind=kOutput, calls=%fused_computation.71 | convolution fusion | flops 805502976 | bytes 5242880 | tf_op jit(solution)/shard_map/dot_general | solution.py:145
  343.9 12.3 %all-gather.8.cloned.1.call-done = bf16[384,2048]{1,0:T(8,128)(2,1)} async-done(((bf16[384,512]{1,0:T(8,128)(2,1)}), bf16[384,2048]{1,0:T(8,128)(2,1)}) %all-gather.8.cloned.1.call-update) | async-done | bytes 1572880 | tf_op jit(solution)/shard_map/all_gather | solution.py:142
  356.2 4.2 %fusion.36 = bf16[384,512]{1,0:T(8,128)(2,1)} fusion(f32[384,512]{1,0:T(8,128)} %convolution_multiply_fusion, f32[384,512]{1,0:T(8,128)} %fusion.29, bf16[384,2048]{1,0:T(8,128)(2,1)} %all-gather.8.cloned.1.call-done, bf16[2048,512]{1,0:T(8,128)(2,1)} %param.26), kind=kOutput, calls=%fused_computation.82 | convolution fusion | flops 805896192 | bytes 5636096 | tf_op jit(solution)/shard_map/dot_general | solution.py:144
  (96 shorter events, 4.9 us)
Async XLA Ops:
  7.2 25.2 %copy-start = (bf16[2048,512]{1,0:T(8,128)(2,1)S(1)}, bf16[2048,512]{1,0:T(8,128)(2,1)}, u32[]{:S(2)}) copy-start(bf16[2048,512]{1,0:T(8,128)(2,1)} %param.22) | copy-start | bytes 6291460
  7.2 23.4 %all-gather.6.cloned.1.call-start = ((), (), s32[]{:S(2)}) async-start(), calls=%async_computation | async-start | bytes 1966080 | tf_op jit(solution)/shard_map/all_gather | solution.py:63
  7.9 85.0 %all-gather.10.cloned.1.call-start = ((), (), s32[]{:S(2)}) async-start(), calls=%async_computation.2 | async-start | bytes 3538944 | tf_op jit(solution)/shard_map/all_gather | solution.py:99
  32.3 3.3 copy-start.8
  35.6 4.1 %copy-start.2 = (bf16[384,2048]{1,0:T(8,128)(2,1)S(1)}, bf16[384,2048]{1,0:T(8,128)(2,1)}, u32[]{:S(2)}) copy-start(bf16[384,2048]{1,0:T(8,128)(2,1)} %all-gather.6.cloned.1.call-done) | copy-start | bytes 4718596
  35.6 118.2 %all-gather.12.cloned.1.call-start = ((), (), s32[]{:S(2)}) async-start(), calls=%async_computation.3 | async-start | bytes 3538944 | tf_op jit(solution)/shard_map/all_gather | solution.py:98
  39.6 300.2 %all-gather.14.cloned.1.call-start = ((), (), s32[]{:S(2)}) async-start(), calls=%async_computation.4 | async-start | bytes 1966080 | tf_op jit(solution)/shard_map/all_gather | solution.py:143
  96.8 61.0 %copy-start.5 = (f32[8]{0:T(128)S(1)}, f32[8]{0:T(128)}, u32[]{:S(2)}) copy-start(f32[8]{0:T(128)} %param.23) | copy-start | bytes 100
  157.8 155.1 %copy-start.4 = (bf16[31,512]{1,0:T(8,128)(2,1)S(1)}, bf16[31,512]{1,0:T(8,128)(2,1)}, u32[]{:S(2)}) copy-start(bf16[31,512]{1,0:T(8,128)(2,1)} %param.24) | copy-start | bytes 95236
  312.6 43.6 %all-gather.8.cloned.1.call-start = ((), (), s32[]{:S(2)}) async-start(), calls=%async_computation.1 | async-start | bytes 1966080 | tf_op jit(solution)/shard_map/all_gather | solution.py:142
  313.0 3.4 copy-start.3
  313.0 3.4 copy-start.6
  317.4 4.7 %collective-permute-start = (bf16[30,512]{1,0:T(8,128)(2,1)S(1)}, bf16[30,512]{1,0:T(8,128)(2,1)S(1)}, u32[]{:S(2)}, u32[]{:S(2)}) collective-permute-start(bf16[30,512]{1,0:T(8,128)(2,1)S(1)} %slice.270), channel_id=1, source_target_pairs={{0,4},{4,8},{8,12},{12,16},{16,20},{20,24},{24,28},{1,5},{5,9},{9,... | collective-permute-start | bytes 92168 | tf_op jit(solution)/shard_map/ppermute | solution.py:16
  334.3 2.9 copy-start.7
  339.8 20.6 %copy-start.1 = (bf16[2048,512]{1,0:T(8,128)(2,1)S(1)}, bf16[2048,512]{1,0:T(8,128)(2,1)}, u32[]{:S(2)}) copy-start(bf16[2048,512]{1,0:T(8,128)(2,1)} %param.22) | copy-start | bytes 6291460
Sparse Core Ops, SparseCore 0:
  9.5 20.9 all-gather.5
  35.7 57.1 all-gather.9
  95.1 58.6 all-gather.11
  312.8 21.2 all-gather.13
  335.4 20.7 all-gather.7
where the time goes:
time: 369 us; the launch traced here: 367 us
  waiting for transfers between devices  146 us (40%)
  other arithmetic  103 us (28%)
  matrix products  67.6 us (18%)
  local copies, waits for them, and re-layouts  26.6 us (7%)
  between operations  14 us (4%)
  blocking collectives  7.28 us (2%)
    another operation x12, other arithmetic  91.3 us
    all_gather x1, waiting for transfers between devices, body(): lax.all_gather(keys, 'sp', axis=0, tiled=True)  57 us
    all_gather x1, waiting for transfers between devices, body(): lax.all_gather(values, 'sp', axis=0, tiled=True)  50.4 us
    dot_general x6, matrix products, sweep_block(): jnp.einsum('thd,shd->hts', query_heads, key_heads, preferred_element_type...  28.2 us
    all_gather x1, waiting for transfers between devices, body(): whole_rows = lax.all_gather(tokens, 'tp', axis=1, tiled=True)  22.6 us
    all_gather x1, waiting for transfers between devices, body(): conv_piece = lax.all_gather(conv_act, 'tp', axis=1, tiled=True)  12.3 us
    dot_general x6, matrix products, sweep_block(): jnp.einsum('hts,shd->thd', stick, value_heads, preferred_element_type=jnp...  12 us
    dynamic_slice x12, local copies, waits for them, and re-layouts, advance(): lax.dynamic_slice_in_dim(all_keys, key_first + key_span, key_span, 0)  8.92 us
  transfers between devices with their start and end apart: 6, of which 5 were waited for; matrix products, arithmetic and copies ran while one was open for 8% of the time, Pallas kernels for 0%

commit v1 on v0

--- a/solution.py
+++ b/solution.py
@@ -1,6 +1,10 @@
+import functools
+
 import jax
 import jax.numpy as jnp
 from jax import lax
+from jax.experimental import pallas as pl
+from jax.experimental.pallas import tpu as pltpu
 from jax.sharding import PartitionSpec as P
 
 HEAD = 64
@@ -42,6 +46,178 @@
         "hts,shd->thd", stick, value_heads, preferred_element_type=jnp.float32
     )
     return (summed, spent_stick + behind[:, :, 0])
+
+
+def softplus_parts(z):
+    x = jnp.exp(-jnp.abs(z))
+    tail = jnp.where(x < 0.004, x - (0.5 * x) * x, jnp.log(1.0 + x))
+    return jnp.maximum(z, 0.0) + tail, jnp.minimum(z, 0.0) - tail
+
+
+def stick_kernel(
+    query_span, strip, cell, width, scale, offset_ref, packed_ref, out_ref, spent_ref,
+    query_s, key_s, value_s, acc_s, carry_s
+):
+    block = pl.program_id(1)
+
+    @pl.when(block == 0)
+    def _():
+        query_s[...] = packed_ref[0, :, :width]
+        key_s[...] = packed_ref[0, :, width : 2 * width]
+        value_s[...] = packed_ref[0, :, 2 * width :]
+
+    offset = offset_ref[0, pl.program_id(0)]
+    later = (
+        lax.broadcasted_iota(jnp.int32, (cell, cell), 0)
+        > lax.broadcasted_iota(jnp.int32, (cell, cell), 1)
+    ).astype(jnp.bfloat16)
+    acc_s[...] = jnp.zeros_like(acc_s)
+    carry_s[...] = jnp.zeros_like(carry_s)
+    query_first = pl.multiple_of(block * query_span, query_span)
+
+    def one(row, key_first, diagonal):
+        rows = pl.ds(row, strip)
+        query = query_s[pl.ds(query_first + row, strip), :]
+        keys = key_s[pl.ds(key_first, cell), :]
+        z = (
+            lax.dot_general(
+                query, keys, (((1,), (1,)), ((), ())), preferred_element_type=jnp.float32
+            )
+            * scale
+            + offset
+        )
+        soft, own = softplus_parts(z)
+        if diagonal:
+            allowed = lax.broadcasted_iota(jnp.int32, z.shape, 1) <= lax.broadcasted_iota(
+                jnp.int32, z.shape, 0
+            )
+            soft = jnp.where(allowed, soft, 0.0)
+        behind = jnp.dot(soft.astype(jnp.bfloat16), later, preferred_element_type=jnp.float32)
+        carry = carry_s[rows, :]
+        stick = jnp.exp(own - behind - carry)
+        if diagonal:
+            stick = jnp.where(allowed, stick, 0.0)
+        acc_s[rows, :] += jnp.dot(
+            stick.astype(jnp.bfloat16),
+            value_s[pl.ds(key_first, cell), :],
+            preferred_element_type=jnp.float32,
+        )
+        carry_s[rows, :] = carry + jnp.sum(soft, axis=1, keepdims=True)
+
+    for col in range(query_span - cell, -1, -cell):
+        for row in range(col, query_span, strip):
+            one(row, query_first + col, row == col)
+
+    def turn(index, _):
+        first = pl.multiple_of(query_first - (index + 1) * query_span, query_span)
+        for col in range(query_span - cell, -1, -cell):
+            for row in range(0, query_span, strip):
+                one(row, first + col, False)
+        return 0
+
+    lax.fori_loop(0, block, turn, 0)
+    out_ref[0] = acc_s[...].astype(out_ref.dtype)
+    spent_ref[0] = jnp.transpose(jnp.broadcast_to(carry_s[...], (query_span, 128)))[:1]
+
+
+def stick_attention(packed, offsets, scale):
+    heads, positions, wide = packed.shape
+    width = wide // 3
+    cell = next(c for c in (256, 128, 64, 32, 16, 8, positions) if positions % c == 0)
+    query_span = 2 * cell if positions % (2 * cell) == 0 else cell
+    out, spent = pl.pallas_call(
+        functools.partial(stick_kernel, query_span, cell, cell, width, scale),
+        grid=(heads, positions // query_span),
+        in_specs=[
+            pl.BlockSpec(memory_space=pltpu.SMEM),
+            pl.BlockSpec((1, positions, wide), lambda h, b: (h, 0, 0)),
+        ],
+        out_specs=[
+            pl.BlockSpec((1, query_span, width), lambda h, b: (h, b, 0)),
+            pl.BlockSpec((1, 1, query_span), lambda h, b: (h, 0, b)),
+        ],
+        out_shape=[
+            jax.ShapeDtypeStruct((heads, positions, width), jnp.bfloat16),
+            jax.ShapeDtypeStruct((heads, 1, positions), jnp.float32),
+        ],
+        scratch_shapes=[
+            pltpu.VMEM((positions, width), jnp.bfloat16),
+            pltpu.VMEM((positions, width), jnp.bfloat16),
+            pltpu.VMEM((positions, width), jnp.bfloat16),
+            pltpu.VMEM((query_span, width), jnp.float32),
+            pltpu.VMEM((query_span, 1), jnp.float32),
+        ],
+        compiler_params=pltpu.CompilerParams(
+            dimension_semantics=("arbitrary", "arbitrary"), vmem_limit_bytes=32 << 20
+        ),
+        cost_estimate=pl.CostEstimate(
+            flops=6 * heads * positions * positions * width,
+            bytes_accessed=8 * heads * positions * width,
+            transcendentals=3 * heads * positions * positions // 2,
+        ),
+    )(offsets, packed)
+    return out, spent[:, 0]
+
+
+def exchanged_attention(queries, keys, values, score_offset, score_scale):
+    tok_rows, columns = queries.shape
+    length = lax.axis_size("sp")
+    head_count = score_offset.shape[0]
+    own_heads = head_count // length
+    width = columns // head_count
+    packed = jnp.stack([queries, keys, values], axis=1)
+    packed = packed.reshape(tok_rows, 3, length, own_heads, width).transpose(2, 3, 0, 1, 4)
+    packed = packed.reshape(length, own_heads, tok_rows, 3 * width)
+    packed = lax.all_to_all(packed, "sp", 0, 0)
+    packed = packed.transpose(1, 0, 2, 3).reshape(own_heads, length * tok_rows, 3 * width)
+    own = lax.dynamic_slice_in_dim(score_offset, lax.axis_index("sp") * own_heads, own_heads, 0)
+    out, spent = stick_attention(packed, own[None], score_scale)
+    out = out.reshape(own_heads, length, tok_rows, width).transpose(1, 0, 2, 3)
+    spent = spent.reshape(own_heads, length, tok_rows).transpose(1, 0, 2)
+    out = lax.all_to_all(out, "sp", 0, 0)
+    spent = lax.all_to_all(spent, "sp", 0, 0)
+    attended = out.transpose(2, 0, 1, 3).reshape(tok_rows, columns)
+    return attended, spent.reshape(head_count, tok_rows)
+
+
+def gathered_attention(queries, keys, values, score_offset, score_scale):
+    tok_rows = queries.shape[0]
+    head_count = score_offset.shape[0]
+    head_width = queries.shape[1] // head_count
+    query_heads = queries.reshape(tok_rows, head_count, head_width)
+    own_index = lax.axis_index("sp")
+    query_first = own_index * tok_rows
+    start_state = (
+        jnp.zeros((tok_rows, head_count, head_width), jnp.float32),
+        jnp.zeros((head_count, tok_rows), jnp.float32),
+    )
+    gathered = (
+        lax.all_gather(keys, "sp", axis=0, tiled=True),
+        lax.all_gather(values, "sp", axis=0, tiled=True),
+    )
+    leading = jnp.zeros((key_span, keys.shape[1]), jnp.bfloat16)
+    all_keys = jnp.concatenate([leading, gathered[0]], axis=0)
+    all_values = jnp.concatenate([leading, gathered[1]], axis=0)
+    key_end = (own_index + 1) * tok_rows
+    turns = (key_end + key_span - 1) // key_span
+
+    def advance(turn_index, sweep_state):
+        key_first = key_end - (turn_index + 1) * key_span
+        key_block = lax.dynamic_slice_in_dim(all_keys, key_first + key_span, key_span, 0)
+        value_block = lax.dynamic_slice_in_dim(all_values, key_first + key_span, key_span, 0)
+        return sweep_block(
+            sweep_state,
+            key_block,
+            value_block,
+            key_first,
+            query_first,
+            query_heads,
+            score_offset,
+            score_scale,
+        )
+
+    summed, spent_stick = lax.fori_loop(0, turns, advance, start_state)
+    return summed.reshape(tok_rows, head_count * head_width).astype(jnp.bfloat16), spent_stick
 
 
 def body(
@@ -86,41 +262,11 @@
     convolved = convolved.astype(jnp.bfloat16)
     head_count = score_offset.shape[0]
     head_width = queries.shape[1] // head_count
-    score_scale = 1.0 / HEAD**0.5
-    query_heads = queries.reshape(tok_rows, head_count, head_width)
-    own_index = lax.axis_index("sp")
-    query_first = own_index * tok_rows
-    start_state = (
-        jnp.zeros((tok_rows, head_count, head_width), jnp.float32),
-        jnp.zeros((head_count, tok_rows), jnp.float32),
-    )
-    gathered = (
-        lax.all_gather(keys, "sp", axis=0, tiled=True),
-        lax.all_gather(values, "sp", axis=0, tiled=True),
-    )
-    leading = jnp.zeros((key_span, keys.shape[1]), jnp.bfloat16)
-    all_keys = jnp.concatenate([leading, gathered[0]], axis=0)
-    all_values = jnp.concatenate([leading, gathered[1]], axis=0)
-    key_end = (own_index + 1) * tok_rows
-    turns = (key_end + key_span - 1) // key_span
-
-    def advance(turn_index, sweep_state):
-        key_first = key_end - (turn_index + 1) * key_span
-        key_block = lax.dynamic_slice_in_dim(all_keys, key_first + key_span, key_span, 0)
-        value_block = lax.dynamic_slice_in_dim(all_values, key_first + key_span, key_span, 0)
-        return sweep_block(
-            sweep_state,
-            key_block,
-            value_block,
-            key_first,
-            query_first,
-            query_heads,
-            score_offset,
-            score_scale,
-        )
-
-    summed, spent_stick = lax.fori_loop(0, turns, advance, start_state)
-    attended = summed.reshape(tok_rows, head_count * head_width).astype(jnp.bfloat16)
+    score_scale = 1.0 / head_width**0.5
+    attention = (
+        exchanged_attention if head_count % lax.axis_size("sp") == 0 else gathered_attention
+    )
+    attended, spent_stick = attention(queries, keys, values, score_offset, score_scale)
     log_weight = jnp.log(-jnp.expm1(-spent_stick))
     gate_conv = jax.nn.sigmoid(jnp.dot(normed, w_gate_conv, preferred_element_type=jnp.float32))
     gate_attn = jax.nn.sigmoid(jnp.dot(normed, w_gate_attn, preferred_element_type=jnp.float32))

time: 369 us -> 182 us (0.49)
  other arithmetic: 103 us -> 7.44 us
  waiting for transfers between devices: 146 us -> 55.4 us
  matrix products: 67.6 us -> 29.4 us
  Pallas kernels: 0 us -> 31.5 us
  local copies, waits for them, and re-layouts: 26.6 us -> 7.54 us
  blocking collectives: 7.28 us -> 22.2 us
  starting transfers between devices: 1.71 us -> 12.4 us
    all_gather x2 -> x0, waiting for transfers between devices: 107 us -> none  [the longest x1 57 us: body(): lax.all_gather(keys, 'sp', axis=0, tiled=True)]
    another operation x18 -> x0, other arithmetic: 93.8 us -> none
    dot_general x12 -> x0, matrix products: 40.2 us -> none  [the longest x6 28.2 us: sweep_block(): jnp.einsum('thd,shd->hts', query_heads, key_heads, preferred_element_type...]
    pallas_call x0 -> x1, Pallas kernels: none -> 31.5 us  [stick_attention(): pl.pallas_call(functools.partial(stick_kernel, query_span, cell, cell, wi...]
    all_to_all x0 -> x2, waiting for transfers between devices: none -> 26.4 us  [the longest x1 26.4 us: exchanged_attention(): packed = lax.all_to_all(packed, 'sp', 0, 0)]
    all_to_all x0 -> x1, blocking collectives: none -> 15 us  [exchanged_attention(): out = lax.all_to_all(out, 'sp', 0, 0)]
    all_to_all x0 -> x2, starting transfers between devices: none -> 11.1 us  [the longest x1 5.64 us: exchanged_attention(): spent = lax.all_to_all(spent, 'sp', 0, 0)]
    dynamic_slice x18 -> x1, local copies, waits for them, and re-layouts: 10.2 us -> 0.59 us  [exchanged_attention(): lax.dynamic_slice_in_dim(score_offset, lax.axis_index('sp') * own_heads,...]
  transfers between devices with their start and end apart: 6 -> 6, of which waited for: 5 -> 4; matrix products, arithmetic and copies ran while one was open for 8% -> 13% of each run, Pallas kernels for 0% -> 0%
where the time goes in v1:
time: 182 us; the launch traced here: 180 us
  waiting for transfers between devices  55.4 us (30%)
  Pallas kernels  31.5 us (17%)
  matrix products  29.4 us (16%)
  blocking collectives  22.2 us (12%)
  between operations  14 us (8%)
  starting transfers between devices  12.4 us (7%)
  local copies, waits for them, and re-layouts  7.54 us (4%)
  other arithmetic  7.44 us (4%)
    pallas_call x1, Pallas kernels, stick_attention(): pl.pallas_call(functools.partial(stick_kernel, query_span, cell, cell, wi...  31.5 us
    all_to_all x1, waiting for transfers between devices, exchanged_attention(): packed = lax.all_to_all(packed, 'sp', 0, 0)  26.4 us
    all_gather x1, waiting for transfers between devices, body(): whole_rows = lax.all_gather(tokens, 'tp', axis=1, tiled=True)  22.6 us
    all_to_all x1, blocking collectives, exchanged_attention(): out = lax.all_to_all(out, 'sp', 0, 0)  15 us
    psum x1, blocking collectives, body(): lax.psum((jnp.sum(conv_float, axis=-1, keepdims=True), jnp.sum(conv_float...  7.19 us
    all_to_all x1, starting transfers between devices, exchanged_attention(): spent = lax.all_to_all(spent, 'sp', 0, 0)  5.64 us
    all_to_all x1, starting transfers between devices, exchanged_attention(): packed = lax.all_to_all(packed, 'sp', 0, 0)  5.44 us
    dot_general x1, matrix products, body(): jnp.dot(normed, w_gate_conv, preferred_element_type=jnp.float32)  4.22 us
  transfers between devices with their start and end apart: 6, of which 4 were waited for; matrix products, arithmetic and copies ran while one was open for 13% of the time, Pallas kernels for 0%

profile of v1, /device:TPU:29, one launch (start us, length us, event | category | flops | bytes accessed | tf_op | source)
XLA Modules:
  0.0 180.0 jit_solution(13571302928459536963)
XLA Ops:
  7.2 0.0 copy-start
  7.2 0.0 all-gather.4.cloned.1.call-start
  7.2 0.7 all-gather.4.cloned.1.call-update
  7.9 22.6 %all-gather.4.cloned.1.call-done = bf16[384,2048]{1,0:T(8,128)(2,1)} async-done(((bf16[384,512]{1,0:T(8,128)(2,1)}), bf16[384,2048]{1,0:T(8,128)(2,1)}) %all-gather.4.cloned.1.call-update) | async-done | bytes 1572880 | tf_op jit(solution)/shard_map/all_gather | solution.py:239
  30.5 1.8 fusion
  32.3 0.0 copy-done
  32.3 0.0 copy-start.5
  32.4 2.4 %convolution_convert_fusion = bf16[384,512]{1,0:T(8,128)(2,1)S(1)} fusion(bf16[2048,512]{1,0:T(8,128)(2,1)S(1)} %copy-done, bf16[384,2048]{1,0:T(8,128)(2,1)} %all-gather.4.cloned.1.call-done, f32[2048]{0:T(1024)} %param.15, f32[384]{0:T(512)S(1)} %add_rsqrt_fusion), kind=kOutput, calls=%fused_computation.52 | convolution fusion | flops 808648704 | bytes 4072960 | tf_op jit(solution)/shard_map/dot_general | solution.py:252
  34.8 0.2 copy.34
  35.0 0.0 copy-done.5
  35.0 3.1 %convolution_convert_fusion.1 = bf16[384,512]{1,0:T(8,128)(2,1)S(1)} fusion(bf16[2048,512]{1,0:T(8,128)(2,1)} %param.19, bf16[384,2048]{1,0:T(8,128)(2,1)} %all-gather.4.cloned.1.call-done, f32[2048]{0:T(1024)S(1)} %copy-done.5, f32[384]{0:T(512)S(1)} %add_rsqrt_fusion), kind=kOutput, calls=%fused_computation.53 | convolution fusion | flops 808648704 | bytes 4072960 | tf_op jit(solution)/shard_map/dot_general | solution.py:251
  38.1 0.2 copy.33
  38.4 3.9 %convolution_convert_fusion.2 = bf16[384,512]{1,0:T(8,128)(2,1)} fusion(bf16[2048,512]{1,0:T(8,128)(2,1)} %param.18, bf16[384,2048]{1,0:T(8,128)(2,1)} %all-gather.4.cloned.1.call-done, f32[2048]{0:T(1024)S(1)} %copy-done.5, f32[384]{0:T(512)S(1)} %add_rsqrt_fusion), kind=kOutput, calls=%fused_computation.54 | convolution fusion | flops 808648704 | bytes 4072960 | tf_op jit(solution)/shard_map/dot_general | solution.py:250
  42.2 1.2 copy.32
  43.4 0.2 maximum_bitcast_fusion
  43.6 0.0 copy-start.6
  43.6 1.2 copy.35
  44.8 5.4 %all-to-all-start = ((bf16[8,1,384,192]{2,3,1,0:T(8,128)(2,1)}), bf16[8,1,384,192]{2,3,1,0:T(8,128)(2,1)S(1)}, u32[]{:S(2)}, u32[]{:S(2)}) async-start(bf16[8,1,384,192]{2,3,1,0:T(8,128)(2,1)} %bitcast.37), calls=%async_computation | async-start | bytes 2359296 | tf_op jit(solution)/shard_map/all_to_all | solution.py:171
  50.2 0.0 all-gather.8.cloned.1.call-start
  50.2 0.0 copy-done.6
  50.2 0.6 dynamic_slice.7
  50.8 26.4 %all-to-all-done = bf16[8,1,384,192]{2,3,1,0:T(8,128)(2,1)S(1)} async-done(((bf16[8,1,384,192]{2,3,1,0:T(8,128)(2,1)}), bf16[8,1,384,192]{2,3,1,0:T(8,128)(2,1)S(1)}, u32[]{:S(2)}, u32[]{:S(2)}) %all-to-all-start) | async-done | bytes 1179680 | tf_op jit(solution)/shard_map/all_to_all | solution.py:171
  77.2 1.6 copy.37
  78.7 0.0 copy-start.1
  78.7 1.4 copy-done.1
  80.1 31.5 %shard_map.149 = (bf16[1,3072,64]{2,1,0:T(8,128)(2,1)S(1)}, f32[1,1,3072]{2,1,0:T(1,128)}) custom-call(f32[1,1]{1,0:T(1,128)} %bitcast.31.offset_ref, bf16[1,3072,192]{2,1,0:T(8,128)(2,1)S(1)} %bitcast.61), custom_call_target="tpu_custom_call" | custom-call | flops 3623878656 | bytes 1572864 | tf_op jit(solution)/shard_map/pallas_call | solution.py:128
  111.7 0.0 copy-start.3
  111.7 0.3 copy.38
  112.0 15.0 %all_to_all.15 = bf16[8,1,384,64]{2,3,1,0:T(8,128)(2,1)} all-to-all(bf16[8,1,384,64]{2,3,1,0:T(8,128)(2,1)S(1)} %copy.38), channel_id=1, replica_groups=mesh['sp'=8,'tp'=4] {'sp'}, dimensions={0} | all-to-all | bytes 786432 | tf_op jit(solution)/shard_map/all_to_all | solution.py:177
  127.0 0.0 all-gather.8.cloned.1.call-update
  127.1 0.0 all-gather.6.cloned.1.call-start
  127.1 0.0 copy-done.3
  127.2 0.0 copy-start.2
  127.2 0.0 copy-start.4
  127.2 3.4 %fusion.9 = f32[384,512]{1,0:T(8,128)S(1)} fusion(bf16[2048,512]{1,0:T(8,128)(2,1)} %param.17, bf16[384,2048]{1,0:T(8,128)(2,1)} %all-gather.4.cloned.1.call-done, f32[2048]{0:T(1024)S(1)} %copy-done.5, f32[384]{0:T(512)S(1)} %add_rsqrt_fusion), kind=kOutput, calls=%fused_computation.46 | convolution fusion | flops 809041920 | bytes 4466176 | tf_op jit(solution)/shard_map/dot_general | solution.py:248
  130.6 0.0 copy-done.2
  130.6 0.0 copy-done.4
  130.6 1.0 fusion.13
  131.6 1.3 collective-permute-start
  133.0 0.8 dynamic_slice.6
  133.7 2.6 %collective-permute-done = bf16[30,512]{1,0:T(8,128)(2,1)S(1)} collective-permute-done((bf16[30,512]{1,0:T(8,128)(2,1)S(1)}, bf16[30,512]{1,0:T(8,128)(2,1)S(1)}, u32[]{:S(2)}, u32[]{:S(2)}) %collective-permute-start) | collective-permute-done | bytes 30752 | tf_op jit(solution)/shard_map/ppermute | solution.py:20
  136.3 3.7 %convert_reduce_fusion = (f32[384]{0:T(512)S(1)}, f32[384]{0:T(512)S(1)}, bf16[384,512]{1,0:T(8,128)(2,1)S(1)}) fusion(bf16[384,512]{1,0:T(8,128)(2,1)S(1)} %fusion.13, f32[512]{0:T(512)S(1)} %bitcast.97, bf16[30,512]{1,0:T(8,128)(2,1)S(1)} %collective-permute-done, f32[512]{0:T(512)S(1)} %bitcast.96, f32[512]{0:T(512)S(1)} %bitcast.95, f32[512]{0:T(512)S(1)} %bitcast.94, ...), kind=kLoop, calls=%fused_computation.57 | loop fusion | flops 36764928 | bytes 883712 | tf_op jit(solution)/shard_map/reduce_sum | solution.py:277
  140.1 7.2 %all-reduce = (f32[384,1]{0,1:T(1,128)S(1)}, f32[384,1]{0,1:T(1,128)S(1)}) all-reduce(f32[384,1]{0,1:T(1,128)S(1)} %broadcast_in_dim.12, f32[384,1]{0,1:T(1,128)S(1)} %broadcast_in_dim.13), channel_id=1, replica_groups=mesh['sp'=8,'tp'=4] {'tp'}, use_global_device_ids=true, to_apply=%region_2.0 | all-reduce | flops 768 | bytes 6144 | tf_op jit(solution)/shard_map/psum | solution.py:275
  147.3 1.1 fusion.22
  148.4 0.0 all-gather.6.cloned.1.call-update
  148.4 3.2 %fusion.11 = f32[384,512]{1,0:T(8,128)S(1)} fusion(bf16[2048,512]{1,0:T(8,128)(2,1)} %param.27, bf16[384,2048]{1,0:T(8,128)(2,1)} %all-gather.4.cloned.1.call-done, f32[2048]{0:T(1024)S(1)} %copy-done.5, f32[384]{0:T(512)S(1)} %add_rsqrt_fusion), kind=kOutput, calls=%fused_computation.48 | convolution fusion | flops 809041920 | bytes 4466176 | tf_op jit(solution)/shard_map/dot_general | solution.py:272
  151.6 5.6 %all-to-all-start.2 = ((f32[8,1,384]{2,1,0:T(1,128)}), f32[8,1,384]{2,1,0:T(1,128)S(1)}, u32[]{:S(2)}, u32[]{:S(2)}) async-start(f32[8,1,384]{2,1,0:T(1,128)} %bitcast.43), calls=%async_computation.2 | async-start | bytes 24576 | tf_op jit(solution)/shard_map/all_to_all | solution.py:178
  157.3 4.2 %fusion.7 = f32[384,512]{1,0:T(8,128)} fusion(bf16[2048,512]{1,0:T(8,128)(2,1)} %param.26, bf16[384,2048]{1,0:T(8,128)(2,1)} %all-gather.4.cloned.1.call-done, f32[2048]{0:T(1024)S(1)} %copy-done.5, f32[384]{0:T(512)S(1)} %add_rsqrt_fusion), kind=kOutput, calls=%fused_computation.44 | convolution fusion | flops 809041920 | bytes 4466176 | tf_op jit(solution)/shard_map/dot_general | solution.py:271
  161.5 0.0 all-to-all-done.2
  161.5 0.6 fusion.56
  162.1 0.0 all-gather.8.cloned.1.call-done
  162.1 4.0 %convolution_multiply_fusion = f32[384,512]{1,0:T(8,128)} fusion(f32[384,512]{1,0:T(8,128)S(1)} %fusion.11, bf16[384,2048]{0,1:T(8,128)(2,1)} %all-gather.8.cloned.1.call-done, bf16[2048,512]{1,0:T(8,128)(2,1)} %param.25), kind=kOutput, calls=%fused_computation.40 | convolution fusion | flops 805502976 | bytes 5242880 | tf_op jit(solution)/shard_map/dot_general | solution.py:291
  166.1 3.2 %all-gather.6.cloned.1.call-done = bf16[384,2048]{1,0:T(8,128)(2,1)} async-done(((bf16[384,512]{1,0:T(8,128)(2,1)}), bf16[384,2048]{1,0:T(8,128)(2,1)}) %all-gather.6.cloned.1.call-update) | async-done | bytes 1572880 | tf_op jit(solution)/shard_map/all_gather | solution.py:288
  169.3 4.2 %fusion.14 = bf16[384,512]{1,0:T(8,128)(2,1)} fusion(f32[384,512]{1,0:T(8,128)} %convolution_multiply_fusion, f32[384,512]{1,0:T(8,128)} %fusion.7, bf16[384,2048]{1,0:T(8,128)(2,1)} %all-gather.6.cloned.1.call-done, bf16[2048,512]{1,0:T(8,128)(2,1)} %param.24), kind=kOutput, calls=%fused_computation.51 | convolution fusion | flops 805896192 | bytes 5636096 | tf_op jit(solution)/shard_map/dot_general | solution.py:290
  (7 shorter events, 0.1 us)
Async XLA Ops:
  7.2 25.2 %copy-start = (bf16[2048,512]{1,0:T(8,128)(2,1)S(1)}, bf16[2048,512]{1,0:T(8,128)(2,1)}, u32[]{:S(2)}) copy-start(bf16[2048,512]{1,0:T(8,128)(2,1)} %param.20) | copy-start | bytes 6291460
  7.2 23.4 %all-gather.4.cloned.1.call-start = ((), (), s32[]{:S(2)}) async-start(), calls=%async_computation.3 | async-start | bytes 1966080 | tf_op jit(solution)/shard_map/all_gather | solution.py:239
  32.3 2.7 %copy-start.5 = (f32[2048]{0:T(1024)S(1)}, f32[2048]{0:T(1024)}, u32[]{:S(2)}) copy-start(f32[2048]{0:T(1024)} %param.15) | copy-start | bytes 24580
  43.6 6.6 %copy-start.6 = (f32[8]{0:T(128)S(1)}, f32[8]{0:T(128)}, u32[]{:S(2)}) copy-start(f32[8]{0:T(128)} %param.21) | copy-start | bytes 100
  44.8 32.4 %all-to-all-start = ((bf16[8,1,384,192]{2,3,1,0:T(8,128)(2,1)}), bf16[8,1,384,192]{2,3,1,0:T(8,128)(2,1)S(1)}, u32[]{:S(2)}, u32[]{:S(2)}) async-start(bf16[8,1,384,192]{2,3,1,0:T(8,128)(2,1)} %bitcast.37), calls=%async_computation | async-start | bytes 2359296 | tf_op jit(solution)/shard_map/all_to_all | solution.py:171
  50.2 111.9 %all-gather.8.cloned.1.call-start = ((), (), s32[]{:S(2)}) async-start(), calls=%async_computation.5 | async-start | bytes 1966080 | tf_op jit(solution)/shard_map/all_gather | solution.py:289
  78.7 1.4 copy-start.1
  111.7 15.4 %copy-start.3 = (bf16[31,512]{1,0:T(8,128)(2,1)S(1)}, bf16[31,512]{1,0:T(8,128)(2,1)}, u32[]{:S(2)}) copy-start(bf16[31,512]{1,0:T(8,128)(2,1)} %param.22) | copy-start | bytes 95236
  127.1 42.2 %all-gather.6.cloned.1.call-start = ((), (), s32[]{:S(2)}) async-start(), calls=%async_computation.4 | async-start | bytes 1966080 | tf_op jit(solution)/shard_map/all_gather | solution.py:288
  127.2 3.4 %copy-start.2 = (bf16[384,2048]{1,0:T(8,128)(2,1)S(1)}, bf16[384,2048]{1,0:T(8,128)(2,1)}, u32[]{:S(2)}) copy-start(bf16[384,2048]{1,0:T(8,128)(2,1)} %all-gather.4.cloned.1.call-done) | copy-start | bytes 4718596
  127.2 3.4 %copy-start.4 = (bf16[2048,512]{1,0:T(8,128)(2,1)S(1)}, bf16[2048,512]{1,0:T(8,128)(2,1)}, u32[]{:S(2)}) copy-start(bf16[2048,512]{1,0:T(8,128)(2,1)} %param.16) | copy-start | bytes 6291460
  131.6 4.7 %collective-permute-start = (bf16[30,512]{1,0:T(8,128)(2,1)S(1)}, bf16[30,512]{1,0:T(8,128)(2,1)S(1)}, u32[]{:S(2)}, u32[]{:S(2)}) collective-permute-start(bf16[30,512]{1,0:T(8,128)(2,1)S(1)} %slice.249), channel_id=1, source_target_pairs={{0,4},{4,8},{8,12},{12,16},{16,20},{20,24},{24,28},{1,5},{5,9},{9,... | collective-permute-start | bytes 92168 | tf_op jit(solution)/shard_map/ppermute | solution.py:20
  151.6 9.9 %all-to-all-start.2 = ((f32[8,1,384]{2,1,0:T(1,128)}), f32[8,1,384]{2,1,0:T(1,128)S(1)}, u32[]{:S(2)}, u32[]{:S(2)}) async-start(f32[8,1,384]{2,1,0:T(1,128)} %bitcast.43), calls=%async_computation.2 | async-start | bytes 24576 | tf_op jit(solution)/shard_map/all_to_all | solution.py:178
Sparse Core Ops, SparseCore 0:
  9.5 20.9 all-gather.3
  127.2 20.2 all-gather.7
  149.6 19.6 all-gather.5

commit v2 on v0

--- a/solution.py
+++ b/solution.py
@@ -1,10 +1,17 @@
+import functools
+
 import jax
 import jax.numpy as jnp
 from jax import lax
+from jax.experimental import pallas as pl
+from jax.experimental.pallas import tpu as pltpu
 from jax.sharding import PartitionSpec as P
 
 HEAD = 64
 WIDTH = 31
+LANES = 128
+HALO = 32
+MESH = pl.DeviceIdType.MESH
 
 
 key_span = 512
@@ -44,7 +51,7 @@
     return (summed, spent_stick + behind[:, :, 0])
 
 
-def body(
+def plain_body(
     tokens,
     norm_gain,
     w_glu_value,
@@ -147,6 +154,446 @@
     return (mixed, log_weight)
 
 
+def remote(src, dst, send_sem, recv_sem, where):
+    return pltpu.make_async_remote_copy(
+        src_ref=src, dst_ref=dst, send_sem=send_sem, recv_sem=recv_sem,
+        device_id=where, device_id_type=MESH,
+    )
+
+
+class Spread:
+    def __init__(self, own_ref, whole_ref, send_sem, recv_sem, pass_send, pass_recv):
+        self.count = lax.axis_size("tp")
+        self.me = lax.axis_index("tp")
+        self.partner = self.me + 1 - 2 * (self.me % 2)
+        self.own_ref, self.whole_ref = own_ref, whole_ref
+        self.sems = (send_sem, recv_sem, pass_send, pass_recv)
+        self.far = range(1, self.count // 2)
+
+    def columns(self, index):
+        width = self.own_ref.shape[1]
+        return self.whole_ref.at[:, pl.ds(pl.multiple_of(index * width, width), width)]
+
+    def first(self, step):
+        where = self.partner if step == 0 else (self.me + 2 * step) % self.count
+        return remote(
+            self.own_ref, self.columns(self.me), self.sems[0].at[step], self.sems[1].at[step],
+            {"tp": where},
+        )
+
+    def passing(self, step):
+        held = self.columns((self.me - 2 * step + self.count) % self.count)
+        return remote(
+            held, held, self.sems[2].at[step], self.sems[3].at[step], {"tp": self.partner}
+        )
+
+    def start(self):
+        for step in self.far:
+            self.first(step).start()
+        self.first(0).start()
+
+    def forward(self):
+        for step in self.far:
+            self.first(step).wait_recv()
+            self.passing(step).start()
+
+    def finish(self):
+        self.first(0).wait()
+        for step in self.far:
+            self.first(step).wait_send()
+            self.passing(step).wait()
+
+    @staticmethod
+    def semaphores(count):
+        return [pltpu.SemaphoreType.DMA((count // 2,)) for _ in range(4)]
+
+
+def greet(barrier):
+    tp_count, tp_me = lax.axis_size("tp"), lax.axis_index("tp")
+    others = [{"tp": tp_me + 1 - 2 * (tp_me % 2)}]
+    others += [{"tp": (tp_me + 2 * step) % tp_count} for step in range(1, tp_count // 2)]
+    for other in others:
+        pl.semaphore_signal(barrier, inc=1, device_id=other, device_id_type=MESH)
+    pl.semaphore_wait(barrier, len(others))
+
+
+def token_kernel(own_ref, gain_ref, normed_ref, whole_ref, keep_sem, *sems):
+    spread = Spread(own_ref, whole_ref, *sems)
+    greet(pltpu.get_barrier_semaphore())
+    spread.start()
+    keep = pltpu.make_async_copy(own_ref, spread.columns(spread.me), keep_sem)
+    keep.start()
+    spread.forward()
+    keep.wait()
+    spread.finish()
+    features_count = whole_ref.shape[1]
+    tall = 64
+
+    @pl.loop(0, whole_ref.shape[0] // tall)
+    def _(index):
+        rows = pl.ds(pl.multiple_of(index * tall, tall), tall)
+        features = whole_ref[rows, :].astype(jnp.float32)
+        square = jnp.sum(features * features, axis=-1, keepdims=True) / features_count
+        normed_ref[rows, :] = (features * lax.rsqrt(square + 1e-06) * gain_ref[...]).astype(
+            jnp.bfloat16
+        )
+
+
+def gather_normed(tokens, norm_gain):
+    rows, columns = tokens.shape
+    count = lax.axis_size("tp")
+    return pl.pallas_call(
+        token_kernel,
+        in_specs=[pl.BlockSpec(memory_space=pltpu.VMEM)] * 2,
+        out_specs=pl.BlockSpec(memory_space=pltpu.VMEM),
+        out_shape=jax.ShapeDtypeStruct((rows, columns * count), jnp.bfloat16),
+        scratch_shapes=[
+            pltpu.VMEM((rows, columns * count), jnp.bfloat16), pltpu.SemaphoreType.DMA
+        ] + Spread.semaphores(count),
+        compiler_params=pltpu.CompilerParams(
+            collective_id=0, has_side_effects=True, vmem_limit_bytes=16 << 20
+        ),
+    )(tokens, norm_gain[None])
+
+
+def softplus_parts(z):
+    x = jnp.exp(-jnp.abs(z))
+    tail = jnp.where(x < 0.004, x - (0.5 * x) * x, jnp.log(1.0 + x))
+    return jnp.maximum(z, 0.0) + tail, jnp.minimum(z, 0.0) - tail
+
+
+def branch_kernel(
+    tap_count, scale, offset_ref, packed_ref, normed_ref, value_hbm, gate_hbm, taps_ref, gain_ref,
+    act_ref, attended_ref, spent_ref,
+    chunks, key_s, value_s, query_s, acc_s, carry_s,
+    back_out, back_in, spent_out, spent_in, own_rows,
+    value_w, gate_w, glued_s, halo_s, extended, conv_s, own_act, stat_out, stat_in,
+    weight_sem, keep_sem, chunk_send, chunk_recv, back_send, back_recv, spent_send, spent_recv,
+    halo_send, halo_recv, stat_send, stat_recv, *spread_sems
+):
+    sp_count, me = lax.axis_size("sp"), lax.axis_index("sp")
+    tp_count, tp_me = lax.axis_size("tp"), lax.axis_index("tp")
+    rows, channels = own_rows.shape
+    width = packed_ref.shape[2] // 3
+    cell = LANES
+
+    weights = [
+        pltpu.make_async_copy(hbm, vmem, weight_sem.at[index])
+        for index, (hbm, vmem) in enumerate(((value_hbm, value_w), (gate_hbm, gate_w)))
+    ]
+    for copy in weights:
+        copy.start()
+    barrier = pltpu.get_barrier_semaphore()
+    for step in range(1, sp_count):
+        pl.semaphore_signal(
+            barrier, inc=1, device_id={"sp": (me + step) % sp_count}, device_id_type=MESH
+        )
+    for step in range(1, tp_count):
+        pl.semaphore_signal(
+            barrier, inc=1, device_id={"tp": (tp_me + step) % tp_count}, device_id_type=MESH
+        )
+    pl.semaphore_wait(barrier, sp_count + tp_count - 2)
+
+    def chunk_copy(step):
+        to = (me + step) % sp_count
+        return remote(
+            packed_ref.at[to], chunks.at[me], chunk_send.at[step], chunk_recv.at[step], {"sp": to}
+        )
+
+    for step in range(1, sp_count):
+        chunk_copy(step).start()
+    keep = pltpu.make_async_copy(packed_ref.at[me], chunks.at[me], keep_sem)
+    keep.start()
+
+    for copy in weights:
+        copy.wait()
+    part = 2 * LANES if channels % (2 * LANES) == 0 else channels
+    for first in range(0, channels, part):
+        cols = pl.ds(first, part)
+        value = jnp.dot(normed_ref[...], value_w[:, cols], preferred_element_type=jnp.float32)
+        gate = jnp.dot(normed_ref[...], gate_w[:, cols], preferred_element_type=jnp.float32)
+        glued = (value * jax.nn.sigmoid(gate)).astype(jnp.bfloat16)
+        extended[pl.ds(HALO, rows), cols] = glued.astype(jnp.float32)
+        glued_s[:, cols] = glued[rows - HALO :]
+
+    def halo_copy():
+        return remote(
+            glued_s, halo_s, halo_send, halo_recv, {"sp": (me + 1) % sp_count}
+        )
+
+    @pl.when(me < sp_count - 1)
+    def _():
+        halo_copy().start()
+
+    @pl.when(me == 0)
+    def _():
+        extended[pl.ds(0, HALO), :] = jnp.zeros((HALO, channels), jnp.float32)
+
+    @pl.when(me > 0)
+    def _():
+        halo_copy().wait_recv()
+        extended[pl.ds(0, HALO), :] = halo_s[...].astype(jnp.float32)
+
+    carry_s[...] = jnp.zeros_like(carry_s)
+    acc_s[...] = jnp.zeros_like(acc_s)
+    sums = [jnp.zeros((rows, 1), jnp.float32)] * 2
+    for first in range(0, channels, LANES):
+        cols = pl.ds(first, LANES)
+        conv = jnp.zeros((rows, LANES), jnp.float32)
+        for tap in range(tap_count):
+            weight = taps_ref[tap : tap + 1, cols].astype(jnp.float32)
+            conv = conv + weight * extended[pl.ds(HALO - tap_count + 1 + tap, rows), cols]
+        conv = conv.astype(jnp.bfloat16)
+        conv_s[:, cols] = conv
+        conv = conv.astype(jnp.float32)
+        sums = [
+            sums[0] + jnp.sum(conv, axis=1, keepdims=True),
+            sums[1] + jnp.sum(conv * conv, axis=1, keepdims=True),
+        ]
+    for index in range(2):
+        stat_out[8 * index : 8 * index + 8, :] = jnp.transpose(
+            jnp.broadcast_to(sums[index], (rows, LANES))
+        )[:8]
+
+    def stat_copy(step):
+        return remote(
+            stat_out, stat_in.at[step], stat_send.at[step], stat_recv.at[step],
+            {"tp": (tp_me + step) % tp_count},
+        )
+
+    for step in range(1, tp_count):
+        stat_copy(step).start()
+    total = stat_out[...]
+    for step in range(1, tp_count):
+        stat_copy(step).wait_recv()
+        total = total + stat_in[step]
+    all_channels = channels * tp_count
+    mean = jnp.transpose(jnp.broadcast_to(total[:1], (LANES, rows))) / all_channels
+    square = jnp.transpose(jnp.broadcast_to(total[8:9], (LANES, rows))) / all_channels
+    inverse = lax.rsqrt(square - mean * mean + 1e-05)
+    for first in range(0, channels, LANES):
+        cols = pl.ds(first, LANES)
+        act = (conv_s[:, cols].astype(jnp.float32) - mean) * inverse * gain_ref[:, cols]
+        own_act[:, cols] = (act * jax.nn.sigmoid(act)).astype(jnp.bfloat16)
+
+    act_spread = Spread(own_act, act_ref, *spread_sems[:4])
+    act_spread.start()
+    act_keep = pltpu.make_async_copy(own_act, act_spread.columns(tp_me), keep_sem)
+    keep.wait()
+    act_keep.start()
+    act_keep.wait()
+
+    offset = offset_ref[0, me]
+    side = lax.broadcasted_iota(jnp.int32, (cell, 2 * cell), 0)
+    across = lax.broadcasted_iota(jnp.int32, (cell, 2 * cell), 1)
+    later = ((side > across) | (across >= cell)).astype(jnp.bfloat16)
+
+    def one(row, key_block, col, diagonal):
+        held = pl.ds(row, rows - row)
+        z = (
+            lax.dot_general(
+                query_s[held, :], key_s[key_block, pl.ds(col, cell), :],
+                (((1,), (1,)), ((), ())), preferred_element_type=jnp.float32,
+            )
+            * scale
+            + offset
+        )
+        soft, own = softplus_parts(z)
+        if diagonal:
+            allowed = lax.broadcasted_iota(jnp.int32, z.shape, 1) <= lax.broadcasted_iota(
+                jnp.int32, z.shape, 0
+            )
+            soft = jnp.where(allowed, soft, 0.0)
+        behind = jnp.dot(soft.astype(jnp.bfloat16), later, preferred_element_type=jnp.float32)
+        carry = carry_s[held, :]
+        stick = jnp.exp(own - behind[:, :cell] - carry)
+        if diagonal:
+            stick = jnp.where(allowed, stick, 0.0)
+        acc_s[held, :] += jnp.dot(
+            stick.astype(jnp.bfloat16), value_s[key_block, pl.ds(col, cell), :],
+            preferred_element_type=jnp.float32,
+        )
+        carry_s[held, :] = carry + behind[:, cell:]
+
+    def back_copies(to, source):
+        return (
+            remote(
+                back_out.at[to], back_in.at[source], back_send.at[to], back_recv.at[source],
+                {"sp": to},
+            ),
+            remote(
+                spent_out.at[to], spent_in.at[source], spent_send.at[to], spent_recv.at[source],
+                {"sp": to},
+            ),
+        )
+
+    def block(index, _):
+        @pl.when(index != me)
+        def _():
+            step = (me - index + sp_count) % sp_count
+            remote(
+                packed_ref.at[index], chunks.at[index], chunk_send.at[step], chunk_recv.at[step],
+                {"sp": (me + step) % sp_count},
+            ).wait_recv()
+
+        @pl.when(index == sp_count // 2)
+        def _():
+            act_spread.forward()
+
+        query_s[...] = chunks[index, :, :width]
+        key_s[index] = chunks[index, :, width : 2 * width]
+        value_s[index] = chunks[index, :, 2 * width :]
+        acc_s[...] = jnp.zeros_like(acc_s)
+        carry_s[...] = jnp.zeros_like(carry_s)
+        for col in range(rows - cell, -1, -cell):
+            one(col, index, col, True)
+
+        def turn(back, _):
+            for col in range(rows - cell, -1, -cell):
+                one(0, index - 1 - back, col, False)
+            return 0
+
+        lax.fori_loop(0, index, turn, 0)
+        done = acc_s[...].astype(jnp.bfloat16)
+        spent = jnp.transpose(carry_s[...])[:8]
+
+        @pl.when(index != me)
+        def _():
+            back_out[index] = done
+            spent_out[index] = spent
+            for copy in back_copies(index, me):
+                copy.start()
+
+        @pl.when(index == me)
+        def _():
+            back_in[index] = done
+            spent_in[index] = spent
+
+        return 0
+
+    lax.fori_loop(0, sp_count, block, 0)
+
+    for source in range(sp_count):
+        @pl.when(source != me)
+        def _():
+            for copy in back_copies((2 * me - source + sp_count) % sp_count, source):
+                copy.wait_recv()
+    own_rows[...] = jnp.concatenate([back_in[source] for source in range(sp_count)], axis=1)
+    last_spread = Spread(own_rows, attended_ref, *spread_sems[4:])
+    last_spread.start()
+    last_keep = pltpu.make_async_copy(own_rows, last_spread.columns(tp_me), keep_sem)
+    last_keep.start()
+    for source in range(sp_count):
+        spent_ref[source : source + 1, :] = spent_in[source, :1]
+    for step in range(1, sp_count):
+        chunk_copy(step).wait_send()
+        for copy in back_copies((me + step) % sp_count, me):
+            copy.wait_send()
+    for step in range(1, tp_count):
+        stat_copy(step).wait_send()
+
+    @pl.when(me < sp_count - 1)
+    def _():
+        halo_copy().wait_send()
+
+    act_spread.finish()
+    last_keep.wait()
+    last_spread.forward()
+    last_spread.finish()
+
+
+def branches(packed, normed, w_value, w_gate, taps, gain, offsets, scale):
+    sp_count, rows, wide = packed.shape
+    width = wide // 3
+    tp_count = lax.axis_size("tp")
+    channels = taps.shape[1]
+    bf, f32 = jnp.bfloat16, jnp.float32
+    dma = pltpu.SemaphoreType.DMA
+    vmem = pl.BlockSpec(memory_space=pltpu.VMEM)
+    hbm = pl.BlockSpec(memory_space=pl.ANY)
+    return pl.pallas_call(
+        functools.partial(branch_kernel, taps.shape[0], scale),
+        in_specs=[pl.BlockSpec(memory_space=pltpu.SMEM), vmem, vmem, hbm, hbm, vmem, vmem],
+        out_specs=[vmem, vmem, vmem],
+        out_shape=[
+            jax.ShapeDtypeStruct((rows, channels * tp_count), bf),
+            jax.ShapeDtypeStruct((rows, channels * tp_count), bf),
+            jax.ShapeDtypeStruct((sp_count, rows), f32),
+        ],
+        scratch_shapes=[
+            pltpu.VMEM((sp_count, rows, wide), bf),
+            pltpu.VMEM((sp_count, rows, width), bf),
+            pltpu.VMEM((sp_count, rows, width), bf),
+            pltpu.VMEM((rows, width), bf),
+            pltpu.VMEM((rows, width), f32),
+            pltpu.VMEM((rows, LANES), f32),
+            pltpu.VMEM((sp_count, rows, width), bf),
+            pltpu.VMEM((sp_count, rows, width), bf),
+            pltpu.VMEM((sp_count, 8, rows), f32),
+            pltpu.VMEM((sp_count, 8, rows), f32),
+            pltpu.VMEM((rows, channels), bf),
+            pltpu.VMEM(w_value.shape, bf),
+            pltpu.VMEM(w_gate.shape, bf),
+            pltpu.VMEM((HALO, channels), bf),
+            pltpu.VMEM((HALO, channels), bf),
+            pltpu.VMEM((HALO + rows, channels), f32),
+            pltpu.VMEM((rows, channels), bf),
+            pltpu.VMEM((rows, channels), bf),
+            pltpu.VMEM((16, rows), f32),
+            pltpu.VMEM((tp_count, 16, rows), f32),
+            dma((2,)), dma,
+            dma((sp_count,)), dma((sp_count,)), dma((sp_count,)), dma((sp_count,)),
+            dma((sp_count,)), dma((sp_count,)), dma, dma, dma((tp_count,)), dma((tp_count,)),
+        ] + Spread.semaphores(tp_count) + Spread.semaphores(tp_count),
+        compiler_params=pltpu.CompilerParams(
+            collective_id=1, has_side_effects=True, vmem_limit_bytes=48 << 20
+        ),
+        cost_estimate=pl.CostEstimate(
+            flops=4 * sp_count * sp_count * rows * rows * width,
+            bytes_accessed=8 * w_value.size,
+            transcendentals=2 * sp_count * sp_count * rows * rows,
+        ),
+    )(offsets, packed, normed, w_value, w_gate, taps, gain)
+
+
+def body(
+    tokens, norm_gain, w_glu_value, w_glu_gate, w_query, w_key, w_value, score_offset, conv_taps,
+    conv_gain, w_conv_out, w_attn_out, w_gate_conv, w_gate_attn,
+):
+    sp_count, tp_count = lax.axis_size("sp"), lax.axis_size("tp")
+    rows, channels = tokens.shape[0], w_query.shape[1]
+    head_count = score_offset.shape[0]
+    fits = rows % LANES == 0 and channels % LANES == 0 and conv_taps.shape[0] <= HALO + 1
+    if head_count != sp_count or tp_count % 2 or not fits:
+        return plain_body(
+            tokens, norm_gain, w_glu_value, w_glu_gate, w_query, w_key, w_value, score_offset,
+            conv_taps, conv_gain, w_conv_out, w_attn_out, w_gate_conv, w_gate_attn,
+        )
+    width = channels // head_count
+    normed = gather_normed(tokens, norm_gain)
+    packed = jnp.stack(
+        [
+            jnp.dot(normed, weight, preferred_element_type=jnp.float32)
+            .astype(jnp.bfloat16)
+            .reshape(rows, sp_count, width)
+            for weight in (w_query, w_key, w_value)
+        ],
+        axis=2,
+    ).reshape(rows, sp_count, 3 * width).transpose(1, 0, 2)
+    local_gain = lax.dynamic_slice_in_dim(conv_gain, lax.axis_index("tp") * channels, channels, 0)
+    conv_piece, attn_piece, spent_stick = branches(
+        packed, normed, w_glu_value, w_glu_gate, conv_taps, local_gain[None], score_offset[None],
+        1.0 / width**0.5,
+    )
+    log_weight = jnp.log(-jnp.expm1(-spent_stick))
+    gate_conv = jax.nn.sigmoid(jnp.dot(normed, w_gate_conv, preferred_element_type=jnp.float32))
+    gate_attn = jax.nn.sigmoid(jnp.dot(normed, w_gate_attn, preferred_element_type=jnp.float32))
+    conv_branch = jnp.dot(conv_piece, w_conv_out, preferred_element_type=jnp.float32)
+    attn_branch = jnp.dot(attn_piece, w_attn_out, preferred_element_type=jnp.float32)
+    mixed = (gate_conv * conv_branch + gate_attn * attn_branch).astype(jnp.bfloat16)
+    return (mixed, log_weight)
+
+
 def solution(mesh):
     in_specs = (
         P("sp", "tp"),

time: 369 us -> 147 us (0.40)
  waiting for transfers between devices: 146 us -> 0 us
  Pallas kernels: 0 us -> 122 us
  other arithmetic: 103 us -> 0.78 us
  matrix products: 67.6 us -> 12.8 us
  local copies, waits for them, and re-layouts: 26.6 us -> 10.1 us
  between operations: 14 us -> 0.8 us
  blocking collectives: 7.28 us -> 0 us
    all_gather x5 -> x0, waiting for transfers between devices: 142 us -> none  [the longest x1 57 us: body(): lax.all_gather(keys, 'sp', axis=0, tiled=True)]
    pallas_call x0 -> x2, Pallas kernels: none -> 122 us  [the longest x1 108 us: branches(): pl.pallas_call(functools.partial(branch_kernel, taps.shape[0], scale), in...]
    another operation x18 -> x1, other arithmetic: 93.8 us -> 0.16 us  [body(): jnp.stack([jnp.dot(normed, weight, preferred_element_type=jnp.float32).as...]
    dot_general x17 -> x3, matrix products: 54.4 us -> 7.8 us  [body(): jnp.dot(normed, weight, preferred_element_type=jnp.float32)]
    dynamic_slice x18 -> x0, local copies, waits for them, and re-layouts: 10.2 us -> none  [the longest x12 8.92 us: advance(): lax.dynamic_slice_in_dim(all_keys, key_first + key_span, key_span, 0)]
    concatenate x2 -> x0, local copies, waits for them, and re-layouts: 7.86 us -> none  [the longest x1 3.95 us: body(): all_keys = jnp.concatenate([leading, gathered[0]], axis=0)]
    psum x1 -> x0, blocking collectives: 7.28 us -> none  [body(): lax.psum((jnp.sum(conv_float, axis=-1, keepdims=True), jnp.sum(conv_float...]
    another operation x12 -> x1, local copies, waits for them, and re-layouts: 7.32 us -> 0.12 us  [body(): jnp.stack([jnp.dot(normed, weight, preferred_element_type=jnp.float32).as...]
  transfers between devices with their start and end apart: 6 -> 0, of which waited for: 5 -> 0; matrix products, arithmetic and copies ran while one was open for 8% -> 0% of each run, Pallas kernels for 0% -> 0%
where the time goes in v2:
time: 147 us; the launch traced here: 146 us
  Pallas kernels  122 us (83%)
  matrix products  12.8 us (9%)
  local copies, waits for them, and re-layouts  10.1 us (7%)
    pallas_call x1, Pallas kernels, branches(): pl.pallas_call(functools.partial(branch_kernel, taps.shape[0], scale), in...  108 us
    pallas_call x1, Pallas kernels, gather_normed(): pl.pallas_call(token_kernel, in_specs=[pl.BlockSpec(memory_space=pltpu.VM...  14.2 us
    dot_general x3, matrix products, body(): jnp.dot(normed, weight, preferred_element_type=jnp.float32)  7.8 us
    unnamed x24, local copies, waits for them, and re-layouts  5.96 us

profile of v2, /device:TPU:29, one launch (start us, length us, event | category | flops | bytes accessed | tf_op | source)
XLA Modules:
  0.0 146.2 jit_solution(2422396151438957422)
XLA Ops:
  0.6 0.0 copy-start
  0.6 0.0 copy-start.4
  0.7 1.1 copy-done.4
  1.8 0.0 copy-start.5
  1.8 0.7 copy-done.5
  2.5 14.2 %shard_map.149.normed_ref = bf16[384,2048]{1,0:T(8,128)(2,1)S(1)} custom-call(bf16[384,512]{1,0:T(8,128)(2,1)S(1)} %copy-done.4, f32[1,2048]{1,0:T(1,128)S(1)} %bitcast.23), custom_call_target="tpu_custom_call" | custom-call | tf_op jit(solution)/shard_map/pallas_call | solution.py:245
  16.7 0.0 copy-start.1
  16.7 1.2 copy-done.1
  17.9 0.0 copy-done
  17.9 1.0 convolution_convert_fusion.2
  18.9 0.2 copy.19
  19.1 3.0 %convolution_convert_fusion.1 = bf16[384,512]{1,0:T(8,128)(2,1)S(1)} fusion(bf16[384,2048]{1,0:T(8,128)(2,1)} %copy-done.1, bf16[2048,512]{1,0:T(8,128)(2,1)} %param.19), kind=kOutput, calls=%fused_computation.13 | convolution fusion | flops 805502976 | bytes 4063232 | tf_op jit(solution)/shard_map/dot_general | solution.py:576
  22.1 0.2 copy.20
  22.3 3.8 %convolution_convert_fusion = bf16[384,512]{1,0:T(8,128)(2,1)} fusion(bf16[384,2048]{1,0:T(8,128)(2,1)} %copy-done.1, bf16[2048,512]{1,0:T(8,128)(2,1)} %param.20), kind=kOutput, calls=%fused_computation.12 | convolution fusion | flops 805502976 | bytes 4063232 | tf_op jit(solution)/shard_map/dot_general | solution.py:576
  26.1 1.2 copy.21
  27.3 0.2 pad_maximum_fusion
  27.5 0.1 copy.22
  27.6 0.0 copy-start.6
  27.7 0.0 copy-start.7
  27.7 1.6 %copy.23 = bf16[384,8,192]{2,0,1:T(8,128)(2,1)} copy(bf16[384,8,192]{0,2,1:T(8,128)(2,1)S(1)} %bitcast.26) | data formatting | bytes 2359296 | tf_op jit(solution)/shard_map/reshape | solution.py:582
  29.3 0.8 dynamic_slice.3
  30.0 0.0 copy-done.6
  30.0 0.0 copy-done.7
  30.0 0.0 copy-start.3
  30.0 1.4 copy-done.3
  31.4 0.0 copy-start.2
  31.4 0.0 copy-start.8
  31.4 107.6 %shard_map.150 = (bf16[384,2048]{1,0:T(8,128)(2,1)S(1)}, bf16[384,2048]{1,0:T(8,128)(2,1)S(1)}, f32[8,384]{1,0:T(8,128)S(1)}) custom-call(f32[1,8]{1,0:T(1,128)S(1)} %bitcast.25, bf16[8,384,192]{2,1,0:T(8,128)(2,1)S(1)} %bitcast.22, bf16[384,2048]{1,0:T(8,128)(2,1)} %copy-done.1, bf16[2048,512]{1,0:T(8,128)(2,1)} %value_hbm.1, bf16[2048,512]{1,0:T(8,128)(2,1)} %gate_hbm.1, ...), custom_call_target="tpu_custom_call" | custom-call | flops 2415919104 | bytes 8388608 | tf_op jit(solution)/shard_map/pallas_call | solution.py:514
  139.0 0.0 copy-done.2
  139.0 0.0 copy-done.8
  139.0 0.0 copy-start.9
  139.0 1.1 fusion.5
  140.1 0.5 copy-done.9
  140.6 0.0 copy-start.10
  140.6 1.0 convolution_multiply_fusion
  141.6 0.6 copy-done.10
  142.2 0.0 copy-start.11
  142.2 1.1 fusion.3
  143.3 0.5 copy-done.11
  143.8 1.7 %fusion.7 = bf16[384,512]{1,0:T(8,128)(2,1)} fusion(f32[384,512]{1,0:T(8,128)S(1)} %convolution_multiply_fusion, f32[384,512]{1,0:T(8,128)S(1)} %fusion.3, bf16[384,2048]{1,0:T(8,128)(2,1)S(1)} %get-tuple-element.5, bf16[2048,512]{1,0:T(8,128)(2,1)S(1)} %copy-done.11), kind=kOutput, calls=%fused_computation.11 | convolution fusion | flops 805896192 | bytes 5636096 | tf_op jit(solution)/shard_map/dot_general | solution.py:591
  145.5 0.6 negate_log_fusion
Async XLA Ops:
  0.6 17.2 %copy-start = (bf16[2048,512]{1,0:T(8,128)(2,1)S(1)}, bf16[2048,512]{1,0:T(8,128)(2,1)}, u32[]{:S(2)}) copy-start(bf16[2048,512]{1,0:T(8,128)(2,1)} %param.18) | copy-start | bytes 6291460
  0.6 1.1 copy-start.4
  1.8 0.7 copy-start.5
  16.7 1.2 copy-start.1
  27.6 2.4 %copy-start.6 = (bf16[31,512]{1,0:T(8,128)(2,1)S(1)}, bf16[31,512]{1,0:T(8,128)(2,1)}, u32[]{:S(2)}) copy-start(bf16[31,512]{1,0:T(8,128)(2,1)} %taps_ref.1) | copy-start | bytes 95236
  27.7 2.4 %copy-start.7 = (f32[8]{0:T(128)S(1)}, f32[8]{0:T(128)}, u32[]{:S(2)}) copy-start(f32[8]{0:T(128)} %param.21) | copy-start | bytes 100
  30.0 1.4 copy-start.3
  31.4 107.6 %copy-start.2 = (bf16[384,2048]{1,0:T(8,128)(2,1)S(1)}, bf16[384,2048]{1,0:T(8,128)(2,1)}, u32[]{:S(2)}) copy-start(bf16[384,2048]{1,0:T(8,128)(2,1)} %copy-done.1) | copy-start | bytes 4718596
  31.4 107.6 %copy-start.8 = (bf16[2048,512]{1,0:T(8,128)(2,1)S(1)}, bf16[2048,512]{1,0:T(8,128)(2,1)}, u32[]{:S(2)}) copy-start(bf16[2048,512]{1,0:T(8,128)(2,1)} %param.27) | copy-start | bytes 6291460
  139.0 1.6 %copy-start.9 = (bf16[2048,512]{1,0:T(8,128)(2,1)S(1)}, bf16[2048,512]{1,0:T(8,128)(2,1)}, u32[]{:S(2)}) copy-start(bf16[2048,512]{1,0:T(8,128)(2,1)} %param.25) | copy-start | bytes 6291460
  140.6 1.6 %copy-start.10 = (bf16[2048,512]{1,0:T(8,128)(2,1)S(1)}, bf16[2048,512]{1,0:T(8,128)(2,1)}, u32[]{:S(2)}) copy-start(bf16[2048,512]{1,0:T(8,128)(2,1)} %param.26) | copy-start | bytes 6291460
  142.2 1.6 %copy-start.11 = (bf16[2048,512]{1,0:T(8,128)(2,1)S(1)}, bf16[2048,512]{1,0:T(8,128)(2,1)}, u32[]{:S(2)}) copy-start(bf16[2048,512]{1,0:T(8,128)(2,1)} %param.24) | copy-start | bytes 6291460

commit v3 on v2

--- a/solution.py
+++ b/solution.py
@@ -274,7 +274,8 @@
     sp_count, me = lax.axis_size("sp"), lax.axis_index("sp")
     tp_count, tp_me = lax.axis_size("tp"), lax.axis_index("tp")
     rows, channels = own_rows.shape
-    width = packed_ref.shape[2] // 3
+    width = packed_ref.shape[2] // 2
+    half = rows // 2
     cell = LANES
 
     weights = [
@@ -300,7 +301,7 @@
             packed_ref.at[to], chunks.at[me], chunk_send.at[step], chunk_recv.at[step], {"sp": to}
         )
 
-    for step in range(1, sp_count):
+    for step in sorted(range(1, sp_count), key=lambda step: abs(step - sp_count // 2)):
         chunk_copy(step).start()
     keep = pltpu.make_async_copy(packed_ref.at[me], chunks.at[me], keep_sem)
     keep.start()
@@ -440,9 +441,10 @@
         def _():
             act_spread.forward()
 
-        query_s[...] = chunks[index, :, :width]
-        key_s[index] = chunks[index, :, width : 2 * width]
-        value_s[index] = chunks[index, :, 2 * width :]
+        query_s[...] = chunks[index, :rows, :width]
+        key_s[index] = chunks[index, :rows, width:]
+        value_s[index, :half] = chunks[index, rows:, :width]
+        value_s[index, half:] = chunks[index, rows:, width:]
         acc_s[...] = jnp.zeros_like(acc_s)
         carry_s[...] = jnp.zeros_like(carry_s)
         for col in range(rows - cell, -1, -cell):
@@ -454,7 +456,7 @@
             return 0
 
         lax.fori_loop(0, index, turn, 0)
-        done = acc_s[...].astype(jnp.bfloat16)
+        done = jnp.concatenate([acc_s[:half, :], acc_s[half:, :]], axis=1).astype(jnp.bfloat16)
         spent = jnp.transpose(carry_s[...])[:8]
 
         @pl.when(index != me)
@@ -478,7 +480,14 @@
         def _():
             for copy in back_copies((2 * me - source + sp_count) % sp_count, source):
                 copy.wait_recv()
-    own_rows[...] = jnp.concatenate([back_in[source] for source in range(sp_count)], axis=1)
+    for part in range(2):
+        own_rows[part * half : (part + 1) * half, :] = jnp.concatenate(
+            [
+                back_in[source][:, part * width : (part + 1) * width]
+                for source in range(sp_count)
+            ],
+            axis=1,
+        )
     last_spread = Spread(own_rows, attended_ref, *spread_sems[4:])
     last_spread.start()
     last_keep = pltpu.make_async_copy(own_rows, last_spread.columns(tp_me), keep_sem)
@@ -503,8 +512,9 @@
 
 
 def branches(packed, normed, w_value, w_gate, taps, gain, offsets, scale):
-    sp_count, rows, wide = packed.shape
-    width = wide // 3
+    sp_count, tall, wide = packed.shape
+    width = wide // 2
+    rows = normed.shape[0]
     tp_count = lax.axis_size("tp")
     channels = taps.shape[1]
     bf, f32 = jnp.bfloat16, jnp.float32
@@ -521,14 +531,14 @@
             jax.ShapeDtypeStruct((sp_count, rows), f32),
         ],
         scratch_shapes=[
-            pltpu.VMEM((sp_count, rows, wide), bf),
+            pltpu.VMEM((sp_count, tall, wide), bf),
             pltpu.VMEM((sp_count, rows, width), bf),
             pltpu.VMEM((sp_count, rows, width), bf),
             pltpu.VMEM((rows, width), bf),
             pltpu.VMEM((rows, width), f32),
             pltpu.VMEM((rows, LANES), f32),
-            pltpu.VMEM((sp_count, rows, width), bf),
-            pltpu.VMEM((sp_count, rows, width), bf),
+            pltpu.VMEM((sp_count, rows // 2, wide), bf),
+            pltpu.VMEM((sp_count, rows // 2, wide), bf),
             pltpu.VMEM((sp_count, 8, rows), f32),
             pltpu.VMEM((sp_count, 8, rows), f32),
             pltpu.VMEM((rows, channels), bf),
@@ -571,15 +581,19 @@
         )
     width = channels // head_count
     normed = gather_normed(tokens, norm_gain)
-    packed = jnp.stack(
+    query, key, value = (
+        jnp.dot(normed, weight, preferred_element_type=jnp.float32)
+        .astype(jnp.bfloat16)
+        .reshape(rows, sp_count, width)
+        for weight in (w_query, w_key, w_value)
+    )
+    packed = jnp.concatenate(
         [
-            jnp.dot(normed, weight, preferred_element_type=jnp.float32)
-            .astype(jnp.bfloat16)
-            .reshape(rows, sp_count, width)
-            for weight in (w_query, w_key, w_value)
+            jnp.concatenate([query, key], axis=2),
+            jnp.concatenate([value[: rows // 2], value[rows // 2 :]], axis=2),
         ],
-        axis=2,
-    ).reshape(rows, sp_count, 3 * width).transpose(1, 0, 2)
+        axis=0,
+    ).transpose(1, 0, 2)
     local_gain = lax.dynamic_slice_in_dim(conv_gain, lax.axis_index("tp") * channels, channels, 0)
     conv_piece, attn_piece, spent_stick = branches(
         packed, normed, w_glu_value, w_glu_gate, conv_taps, local_gain[None], score_offset[None],

time: 147 us -> 138 us (0.939)
  Pallas kernels: 122 us -> 111 us
  other arithmetic: 0.78 us -> 2.88 us
    pallas_call x1, Pallas kernels: 108 us -> 96.7 us  [branches(): pl.pallas_call(functools.partial(branch_kernel, taps.shape[0], scale), in...]
    transpose x0 -> x1, other arithmetic: none -> 2.26 us  [body(): packed = jnp.concatenate([jnp.concatenate([query, key], axis=2), jnp.conc...]
    slice x0 -> x5, local copies, waits for them, and re-layouts: none -> 2.13 us  [the longest x3 1.08 us: body(): value[:rows // 2]]
    unnamed x24 -> x22, local copies, waits for them, and re-layouts: 5.96 us -> 4.98 us
where the time goes in v3:
time: 138 us; the launch traced here: 137 us
  Pallas kernels  111 us (80%)
  matrix products  12 us (9%)
  local copies, waits for them, and re-layouts  10.6 us (8%)
  other arithmetic  2.88 us (2%)
    pallas_call x1, Pallas kernels, branches(): pl.pallas_call(functools.partial(branch_kernel, taps.shape[0], scale), in...  96.7 us
    pallas_call x1, Pallas kernels, gather_normed(): pl.pallas_call(token_kernel, in_specs=[pl.BlockSpec(memory_space=pltpu.VM...  14.2 us
    dot_general x3, matrix products, body(): jnp.dot(normed, weight, preferred_element_type=jnp.float32)  7.05 us
    unnamed x22, local copies, waits for them, and re-layouts  4.98 us

profile of v3, /device:TPU:29, one launch (start us, length us, event | category | flops | bytes accessed | tf_op | source)
XLA Modules:
  0.0 137.3 jit_solution(10733192278059547475)
XLA Ops:
  0.6 0.0 copy-start
  0.6 0.0 copy-start.3
  0.7 1.1 copy-done.3
  1.8 0.0 copy-start.4
  1.8 0.7 copy-done.4
  2.5 14.2 %shard_map.149.normed_ref = bf16[384,2048]{1,0:T(8,128)(2,1)S(1)} custom-call(bf16[384,512]{1,0:T(8,128)(2,1)S(1)} %copy-done.3, f32[1,2048]{1,0:T(1,128)S(1)} %bitcast.23), custom_call_target="tpu_custom_call" | custom-call | tf_op jit(solution)/shard_map/pallas_call | solution.py:245
  16.7 0.0 copy-done
  16.7 0.0 copy-start.1
  16.7 1.0 convolution_convert_fusion
  17.7 0.2 copy-done.1
  17.9 0.1 copy.20
  18.1 0.9 copy.22
  19.0 0.1 copy.21
  19.1 0.9 copy.23
  20.0 3.0 %convolution_convert_fusion.2 = bf16[384,512]{1,0:T(8,128)(2,1)S(1)} fusion(bf16[384,2048]{1,0:T(8,128)(2,1)} %copy-done.1, bf16[2048,512]{1,0:T(8,128)(2,1)} %param.18), kind=kOutput, calls=%fused_computation.14 | convolution fusion | flops 805502976 | bytes 4063232 | tf_op jit(solution)/shard_map/dot_general | solution.py:585
  23.1 0.2 copy.16
  23.3 1.2 copy.18
  24.5 3.0 %convolution_convert_fusion.1 = bf16[384,512]{1,0:T(8,128)(2,1)S(1)} fusion(bf16[384,2048]{1,0:T(8,128)(2,1)} %copy-done.1, bf16[2048,512]{1,0:T(8,128)(2,1)} %param.19), kind=kOutput, calls=%fused_computation.13 | convolution fusion | flops 805502976 | bytes 4063232 | tf_op jit(solution)/shard_map/dot_general | solution.py:585
  27.5 0.2 copy.17
  27.7 0.0 copy-start.5
  27.8 0.0 copy-start.6
  27.8 1.2 copy.19
  28.9 2.3 %maximum_bitcast_fusion.packed_ref = bf16[8,576,128]{2,1,0:T(8,128)(2,1)S(1)} fusion(bf16[192,8,64]{2,0,1:T(8,128)(2,1)} %copy.23, bf16[192,8,64]{2,0,1:T(8,128)(2,1)} %copy.22, bf16[384,8,64]{2,0,1:T(8,128)(2,1)} %copy.19, bf16[384,8,64]{2,0,1:T(8,128)(2,1)} %copy.18), kind=kLoop, calls=%fused_computation.15 | loop fusion | flops 4718592 | bytes 2359296 | tf_op jit(solution)/shard_map/transpose | solution.py:596
  31.2 0.8 dynamic_slice.3
  32.0 0.0 copy-done.5
  32.0 0.0 copy-done.6
  32.0 0.0 copy-start.2
  32.0 1.4 %copy-done.2 = bf16[384,2048]{1,0:T(8,128)(2,1)S(1)} copy-done((bf16[384,2048]{1,0:T(8,128)(2,1)S(1)}, bf16[384,2048]{1,0:T(8,128)(2,1)}, u32[]{:S(2)}) %copy-start.2) | copy-done | bytes 1572888
  33.4 0.0 copy-start.7
  33.4 96.7 %shard_map.150 = (bf16[384,2048]{1,0:T(8,128)(2,1)S(1)}, bf16[384,2048]{1,0:T(8,128)(2,1)S(1)}, f32[8,384]{1,0:T(8,128)S(1)}) custom-call(f32[1,8]{1,0:T(1,128)S(1)} %bitcast.25, bf16[8,576,128]{2,1,0:T(8,128)(2,1)S(1)} %maximum_bitcast_fusion.packed_ref, bf16[384,2048]{1,0:T(8,128)(2,1)S(1)} %copy-done.2, bf16[2048,512]{1,0:T(8,128)(2,1)} %value_hbm.1, ...), custom_call_target="tpu_custom_call" | custom-call | flops 2415919104 | bytes 8388608 | tf_op jit(solution)/shard_map/pallas_call | solution.py:524
  130.1 0.0 copy-done.7
  130.1 0.0 copy-start.8
  130.1 1.1 fusion.5
  131.3 0.5 copy-done.8
  131.7 0.0 copy-start.9
  131.7 1.0 convolution_multiply_fusion
  132.7 0.6 copy-done.9
  133.3 0.0 copy-start.10
  133.3 1.1 fusion.3
  134.4 0.5 copy-done.10
  134.9 1.7 %fusion.7 = bf16[384,512]{1,0:T(8,128)(2,1)} fusion(f32[384,512]{1,0:T(8,128)S(1)} %convolution_multiply_fusion, f32[384,512]{1,0:T(8,128)S(1)} %fusion.3, bf16[384,2048]{1,0:T(8,128)(2,1)S(1)} %get-tuple-element.5, bf16[2048,512]{1,0:T(8,128)(2,1)S(1)} %copy-done.10), kind=kOutput, calls=%fused_computation.11 | convolution fusion | flops 805896192 | bytes 5636096 | tf_op jit(solution)/shard_map/dot_general | solution.py:605
  136.7 0.6 negate_log_fusion
  (1 shorter events, 0.0 us)
Async XLA Ops:
  0.6 16.1 %copy-start = (bf16[2048,512]{1,0:T(8,128)(2,1)S(1)}, bf16[2048,512]{1,0:T(8,128)(2,1)}, u32[]{:S(2)}) copy-start(bf16[2048,512]{1,0:T(8,128)(2,1)} %param.20) | copy-start | bytes 6291460
  0.6 1.1 copy-start.3
  1.8 0.7 copy-start.4
  16.7 1.2 copy-start.1
  27.7 4.2 %copy-start.5 = (bf16[31,512]{1,0:T(8,128)(2,1)S(1)}, bf16[31,512]{1,0:T(8,128)(2,1)}, u32[]{:S(2)}) copy-start(bf16[31,512]{1,0:T(8,128)(2,1)} %taps_ref.1) | copy-start | bytes 95236
  27.8 4.2 %copy-start.6 = (f32[8]{0:T(128)S(1)}, f32[8]{0:T(128)}, u32[]{:S(2)}) copy-start(f32[8]{0:T(128)} %param.21) | copy-start | bytes 100
  32.0 1.4 %copy-start.2 = (bf16[384,2048]{1,0:T(8,128)(2,1)S(1)}, bf16[384,2048]{1,0:T(8,128)(2,1)}, u32[]{:S(2)}) copy-start(bf16[384,2048]{1,0:T(8,128)(2,1)} %copy-done.1) | copy-start | bytes 4718596
  33.4 96.7 %copy-start.7 = (bf16[2048,512]{1,0:T(8,128)(2,1)S(1)}, bf16[2048,512]{1,0:T(8,128)(2,1)}, u32[]{:S(2)}) copy-start(bf16[2048,512]{1,0:T(8,128)(2,1)} %param.27) | copy-start | bytes 6291460
  130.1 1.6 %copy-start.8 = (bf16[2048,512]{1,0:T(8,128)(2,1)S(1)}, bf16[2048,512]{1,0:T(8,128)(2,1)}, u32[]{:S(2)}) copy-start(bf16[2048,512]{1,0:T(8,128)(2,1)} %param.25) | copy-start | bytes 6291460
  131.7 1.6 %copy-start.9 = (bf16[2048,512]{1,0:T(8,128)(2,1)S(1)}, bf16[2048,512]{1,0:T(8,128)(2,1)}, u32[]{:S(2)}) copy-start(bf16[2048,512]{1,0:T(8,128)(2,1)} %param.26) | copy-start | bytes 6291460
  133.3 1.6 %copy-start.10 = (bf16[2048,512]{1,0:T(8,128)(2,1)S(1)}, bf16[2048,512]{1,0:T(8,128)(2,1)}, u32[]{:S(2)}) copy-start(bf16[2048,512]{1,0:T(8,128)(2,1)} %param.24) | copy-start | bytes 6291460
